TPU v7x, 256 devices: a whole 4x4x8 slice. The times are simulated.
256 devices in a mesh: sp: 32 (over z, x), tp: 8 (over y, core).
Axes of the slice: x: 4, y: 4, z: 8, core: 2. Of those that a mesh axis runs over, the one named last changes fastest.
Arguments:
- layer_input: bfloat16 [16, 16384, 2048], P(None, ('sp', 'tp')), as said below
- key_weight: bfloat16 [2048, 384], replicated, may hold values from -0.125 to 0.125
- value_weight: bfloat16 [2048, 384], replicated, may hold values from -0.125 to 0.125
- queries: bfloat16 [96, 5, 64], P('sp'), may hold values from -6 to 6
- head_bias: float32 [6, 5], replicated, as said below
Outputs:
- stored: bfloat16 [96, 32, 512, 128], P('sp', None, 'tp')
- first_read: bfloat16 [96, 320], P('sp')
Inputs may be any that keep to these rules, and one draw needn't show every extreme that they name: `layer_input`: entries lie between -12.5 and 12.5. `head_bias`: entries lie between -1 minus the natural logarithm of 16384 and -3.
All inputs are finite; a program needn't handle non-finite values.
Results may differ from a plain program's by a relative error of at most 0.01.
Values may be sent and summed in bfloat16 or wider, within the bound.
A program may use at most 64 MiB of HBM per device.

v0:
```python
import math

import jax
import jax.numpy as jnp
from jax import lax
from jax.sharding import PartitionSpec as P

HD = 64
KVH = 6
GROUP = 5


EPS_NORM = 0.0001


def copy_for_each(x, axis):
    count = lax.axis_size(axis)
    return lax.all_to_all(jnp.broadcast_to(x[None], (count, *x.shape)), axis, 0, 0, tiled=True)


def laid_out(tiles, dim):
    tiles = jnp.moveaxis(tiles, 0, dim)
    shape = tiles.shape
    return tiles.reshape(*shape[:dim], shape[dim] * shape[dim + 1], *shape[dim + 2 :])


def collect(x, axis, dim):
    tiles = copy_for_each(x, axis)
    return laid_out(tiles, dim)


def of_everyone(x, axis):
    return copy_for_each(x, axis).sum(axis=0)


def head_norm(summed):
    squares = jnp.mean(summed * summed, axis=-1, keepdims=True)
    return summed * lax.rsqrt(squares + EPS_NORM)


def shift_table(pair_ids, head_bias):
    heads_range = jnp.arange(KVH, dtype=jnp.int32)
    picker = (pair_ids[:, None] % KVH == heads_range[None, :]).astype(jnp.float32)
    return jnp.dot(picker, head_bias, precision=lax.Precision.HIGHEST)


def per_device(layer_input, key_weight, value_weight, queries, head_bias):
    seq_count, positions, model_width = layer_input.shape
    tokens_flat = layer_input.reshape(seq_count * positions, model_width)
    key_rows = (
        jnp.dot(tokens_flat, key_weight, preferred_element_type=jnp.float32)
        .astype(jnp.bfloat16)
        .reshape(seq_count, positions, KVH, HD)
    )
    value_rows = (
        jnp.dot(tokens_flat, value_weight, preferred_element_type=jnp.float32)
        .astype(jnp.bfloat16)
        .reshape(seq_count, positions, KVH, HD)
    )
    kv_rows = (
        jnp.concatenate([key_rows, value_rows], axis=-1)
        .transpose(0, 2, 1, 3)
        .reshape(seq_count * KVH, 1, positions, 2 * HD)
    )
    stored = lax.all_to_all(kv_rows, "sp", split_axis=0, concat_axis=1, tiled=True)
    score_scale = 1.0 / math.sqrt(HD)
    local_pairs = queries.shape[0]
    pair_ids = lax.axis_index("sp") * local_pairs + jnp.arange(local_pairs, dtype=jnp.int32)
    head_shift = shift_table(pair_ids, head_bias)
    scores = (
        jnp.einsum("pgc,pbtc->pgbt", queries, stored[..., :HD], preferred_element_type=jnp.float32)
        * score_scale
        + head_shift[:, :, None, None]
    )
    keep_log = jax.nn.log_sigmoid(-scores)
    totals = jnp.sum(keep_log, axis=3)
    gathered = collect(totals[None], "tp", 0)
    later_mask = (jnp.arange(gathered.shape[0], dtype=jnp.int32) > lax.axis_index("tp")).astype(
        jnp.float32
    )
    later_inside = jnp.sum(gathered * later_mask[:, None, None, None], axis=0)
    block_sums = jnp.sum(gathered, axis=0)
    later_blocks = lax.cumsum(block_sums, axis=2, reverse=True) - block_sums
    suffix_log = (
        lax.cumsum(keep_log, axis=3, reverse=True)
        - keep_log
        + (later_inside + later_blocks)[..., None]
    )
    weights = jnp.exp(jax.nn.log_sigmoid(scores) + suffix_log).astype(jnp.bfloat16)
    partial_value = jnp.einsum(
        "pgbt,pbtc->pgc", weights, stored[..., HD:], preferred_element_type=jnp.float32
    )
    summed = of_everyone(partial_value, "tp")
    first_read = head_norm(summed).reshape(local_pairs, GROUP * HD).astype(jnp.bfloat16)
    return (stored, first_read)


def solution(mesh):
    in_specs = (P(None, ("sp", "tp"), None), P(), P(), P("sp", None, None), P())
    out_specs = (P("sp", None, "tp", None), P("sp", None))
    return jax.shard_map(
        per_device, mesh=mesh, in_specs=in_specs, out_specs=out_specs, check_vma=False
    )
```

profile of v0, /device:TPU:1, one launch (start us, length us, event | category | flops | bytes accessed | tf_op | source)
XLA Modules:
  0.0 116.4 jit_solution(7650277764900114189)
XLA Ops:
  0.6 1.4 %copy-done = bf16[2048,384]{1,0:T(8,128)(2,1)S(1)} copy-done((bf16[2048,384]{1,0:T(8,128)(2,1)S(1)}, bf16[2048,384]{1,0:T(8,128)(2,1)}, u32[]{:S(2)}) %copy-start) | copy-done | bytes 1572888
  2.0 4.5 %convolution_convert_fusion.1 = bf16[1024,384]{1,0:T(8,128)(2,1)S(1)} fusion(bf16[1024,2048]{1,0:T(8,128)(2,1)} %bitcast.45, bf16[2048,384]{1,0:T(8,128)(2,1)S(1)} %copy-done), kind=kOutput, calls=%fused_computation.7 | convolution fusion | flops 1611005952 | bytes 6553600 | tf_op jit(solution)/shard_map/dot_general | solution.py:51
  6.6 1.2 %copy.55 = bf16[1024,384]{0,1:T(8,128)(2,1)} copy(bf16[1024,384]{1,0:T(8,128)(2,1)S(1)} %convolution_convert_fusion.1) | data formatting | bytes 1572864 | tf_op jit(solution)/shard_map/convert_element_type | solution.py:52
  7.7 2.5 %reshape.73 = bf16[16,64,6,64]{1,0,3,2:T(8,128)(2,1)S(1)} reshape(bf16[1024,384]{0,1:T(8,128)(2,1)} %copy.55) | data formatting | bytes 1572864 | tf_op jit(solution)/shard_map/reshape | solution.py:53
  10.2 5.9 %convolution_convert_fusion = bf16[1024,384]{1,0:T(8,128)(2,1)} fusion(bf16[1024,2048]{1,0:T(8,128)(2,1)} %bitcast.46, bf16[2048,384]{1,0:T(8,128)(2,1)} %param.7), kind=kOutput, calls=%fused_computation.6 | convolution fusion | flops 1611005952 | bytes 6553600 | tf_op jit(solution)/shard_map/dot_general | solution.py:56
  16.1 2.3 %copy.56 = bf16[1024,384]{0,1:T(8,128)(2,1)} copy(bf16[1024,384]{1,0:T(8,128)(2,1)} %convolution_convert_fusion) | data formatting | bytes 1572864 | tf_op jit(solution)/shard_map/convert_element_type | solution.py:57
  18.4 3.2 %reshape.74 = bf16[16,64,6,64]{1,0,3,2:T(8,128)(2,1)} reshape(bf16[1024,384]{0,1:T(8,128)(2,1)} %copy.56) | data formatting | bytes 1572864 | tf_op jit(solution)/shard_map/reshape | solution.py:58
  21.6 3.7 %maximum_bitcast_fusion = bf16[16,6,64,128]{2,0,3,1:T(8,128)(2,1)} fusion(bf16[16,64,6,64]{1,0,3,2:T(8,128)(2,1)} %reshape.74, bf16[16,64,6,64]{1,0,3,2:T(8,128)(2,1)S(1)} %reshape.73), kind=kLoop, calls=%fused_computation | loop fusion | flops 786432 | bytes 3145728 | tf_op jit(solution)/shard_map/transpose | solution.py:62
  25.3 5.0 %copy.57 = bf16[16,6,64,128]{3,2,1,0:T(8,128)(2,1)} copy(bf16[16,6,64,128]{2,0,3,1:T(8,128)(2,1)} %maximum_bitcast_fusion) | data formatting | bytes 3145728 | tf_op jit(solution)/shard_map/transpose | solution.py:62
  30.3 12.0 %all-to-all-start = ((bf16[96,1,64,128]{3,2,1,0:T(8,128)(2,1)}), bf16[96,1,64,128]{3,2,1,0:T(8,128)(2,1)S(1)}, u32[]{:S(2)}, u32[]{:S(2)}) async-start(bf16[96,1,64,128]{3,2,1,0:T(8,128)(2,1)} %bitcast.40), calls=%async_computation | async-start | bytes 3145728 | tf_op jit(solution)/shard_map/all_to_all | solution.py:65
  42.3 0.2 fusion.28
  42.5 37.7 %all-to-all-done = bf16[96,1,64,128]{3,2,1,0:T(8,128)(2,1)S(1)} async-done(((bf16[96,1,64,128]{3,2,1,0:T(8,128)(2,1)}), bf16[96,1,64,128]{3,2,1,0:T(8,128)(2,1)S(1)}, u32[]{:S(2)}, u32[]{:S(2)}) %all-to-all-start) | async-done | bytes 1572896 | tf_op jit(solution)/shard_map/all_to_all | solution.py:65
  80.2 0.1 copy.87
  80.3 0.5 copy-done.3
  80.8 2.2 %fusion.21 = (f32[3,5,32]{1,2,0:T(8,128)S(1)}, f32[3,5,32,64]{3,1,2,0:T(8,128)}, f32[3,5,32,64]{3,1,2,0:T(8,128)}) fusion(f32[3,5]{1,0:T(4,128)S(1)} %fusion.28, bf16[3,5,64,1]{2,0,1,3:T(4,128)(2,1)S(1)} %bitcast.47, bf16[3,32,64,128]{3,2,1,0:T(8,128)(2,1)S(1)} %bitcast.41), kind=kOutput, calls=%fused_computation.20 | convolution fusion | flops 4238880 | bytes 1822524 | tf_op jit(solution)/shard_map/pgc,pbtc->pgbt/dot_general | solution.py:71
  83.2 0.5 broadcast.58
  83.7 0.8 reduce.1
  84.5 0.7 reshape.79
  85.2 6.6 %all-to-all-start.1 = ((f32[8,1,480]{2,1,0:T(1,128)}), f32[8,1,480]{2,1,0:T(1,128)S(1)}, u32[]{:S(2)}, u32[]{:S(2)}) async-start(f32[8,1,480]{2,1,0:T(1,128)} %reshape.79), calls=%async_computation.1 | async-start | bytes 32768 | tf_op jit(solution)/shard_map/all_to_all | solution.py:18
  91.9 1.0 copy.61
  92.9 8.3 %reduce_window_sum.20 = f32[3,5,32,64]{3,2,1,0:T(8,128)} reduce-window(f32[3,5,32,64]{3,2,1,0:T(8,128)S(1)} %copy.61, f32[]{:T(128)} %constant.36.clone.1), window={size=1x1x1x64 pad=0_0x0_0x0_0x0_63}, to_apply=%region_0.1 | reduce-window | flops 1935360 | bytes 245764 | tf_op jit(solution)/shard_map/per_device/reduce_window_sum | solution.py:85
  101.2 0.7 reduce.2
  101.9 0.1 reshape.80
  102.1 0.7 reduce_window_sum.21
  102.7 0.1 fusion.26
  102.9 0.1 copy.66
  103.0 2.3 %fusion.13 = f32[3,5,64]{2,1,0:T(8,128)S(1)} fusion(bf16[3,32,64,128]{3,2,1,0:T(8,128)(2,1)S(1)} %bitcast.43, f32[3,5,32,64]{3,2,1,0:T(8,128)} %reduce_window_sum.20, f32[3,5,32,64]{3,1,2,0:T(8,128)} %get-tuple-element.4, f32[3,5,32]{1,2,0:T(8,128)S(1)} %copy.66), kind=kOutput, calls=%fused_computation.13 | convolution fusion | flops 4515840 | bytes 1824384 | tf_op jit(solution)/shard_map/pgbt,pbtc->pgc/dot_general | solution.py:90
  105.3 0.1 reshape.81
  105.4 9.3 %all_to_all.28 = f32[8,1,960]{2,1,0:T(1,128)S(1)} all-to-all(f32[8,1,960]{2,1,0:T(1,128)S(1)} %reshape.81), channel_id=1, replica_groups=mesh['sp'=32,'tp'=8] {'tp'}, dimensions={0} | all-to-all | bytes 61440 | tf_op jit(solution)/shard_map/all_to_all | solution.py:18
  114.7 0.7 reduce.3
  115.4 0.1 reshape.82
  115.8 0.7 convert_element_type.28
  (23 shorter events, 0.5 us)
Async XLA Ops:
  0.6 1.4 %copy-start = (bf16[2048,384]{1,0:T(8,128)(2,1)S(1)}, bf16[2048,384]{1,0:T(8,128)(2,1)}, u32[]{:S(2)}) copy-start(bf16[2048,384]{1,0:T(8,128)(2,1)} %param.6) | copy-start | bytes 4718596
  30.3 12.0 %copy-start.4 = (f32[6,5]{1,0:T(8,128)S(1)}, f32[6,5]{1,0:T(8,128)}, u32[]{:S(2)}) copy-start(f32[6,5]{1,0:T(8,128)} %param.9) | copy-start | bytes 364
  30.3 49.9 %all-to-all-start = ((bf16[96,1,64,128]{3,2,1,0:T(8,128)(2,1)}), bf16[96,1,64,128]{3,2,1,0:T(8,128)(2,1)S(1)}, u32[]{:S(2)}, u32[]{:S(2)}) async-start(bf16[96,1,64,128]{3,2,1,0:T(8,128)(2,1)} %bitcast.40), calls=%async_computation | async-start | bytes 3145728 | tf_op jit(solution)/shard_map/all_to_all | solution.py:65
  80.2 0.7 copy-start.3
  80.3 2.8 %copy-start.1 = (bf16[32,3,1,64,128]{4,3,0,1,2:T(8,128)(2,1)}, bf16[32,3,1,64,128]{4,3,0,1,2:T(8,128)(2,1)S(1)}, u32[]{:S(2)}) copy-start(bf16[32,3,1,64,128]{4,3,0,1,2:T(8,128)(2,1)S(1)} %copy.87) | copy-start | bytes 4718596
  83.1 19.9 %copy-start.2 = (bf16[32,3,1,64,128]{4,3,0,1,2:T(8,128)(2,1)S(1)}, bf16[32,3,1,64,128]{4,3,0,1,2:T(8,128)(2,1)}, u32[]{:S(2)}) copy-start(bf16[32,3,1,64,128]{4,3,0,1,2:T(8,128)(2,1)} %copy-done.1) | copy-start | bytes 4718596
  85.2 16.0 %all-to-all-start.1 = ((f32[8,1,480]{2,1,0:T(1,128)}), f32[8,1,480]{2,1,0:T(1,128)S(1)}, u32[]{:S(2)}, u32[]{:S(2)}) async-start(f32[8,1,480]{2,1,0:T(1,128)} %reshape.79), calls=%async_computation.1 | async-start | bytes 32768 | tf_op jit(solution)/shard_map/all_to_all | solution.py:18
where the time goes:
time: 117 us; the launch traced here: 116 us
  waiting for transfers between devices  37.7 us (32%)
  local copies, waits for them, and re-layouts  19.7 us (17%)
  starting transfers between devices  18.6 us (16%)
  other arithmetic  15.2 us (13%)
  matrix products  15.1 us (13%)
  blocking collectives  9.32 us (8%)
    all_to_all x1, waiting for transfers between devices, per_device(): lax.all_to_all(kv_rows, 'sp', split_axis=0, concat_axis=1, tiled=True)  37.7 us
    all_to_all x1, starting transfers between devices, per_device(): lax.all_to_all(kv_rows, 'sp', split_axis=0, concat_axis=1, tiled=True)  12 us
    all_to_all x1, blocking collectives, copy_for_each(): lax.all_to_all(jnp.broadcast_to(x[None], (count, *x.shape)), axis, 0, 0,...  9.32 us
    another operation x1, other arithmetic, per_device(): lax.cumsum(keep_log, axis=3, reverse=True) - keep_log  8.27 us
    all_to_all x1, starting transfers between devices, copy_for_each(): lax.all_to_all(jnp.broadcast_to(x[None], (count, *x.shape)), axis, 0, 0,...  6.65 us
    dot_general x1, matrix products, per_device(): jnp.dot(tokens_flat, value_weight, preferred_element_type=jnp.float32)  5.88 us
    transpose x1, local copies, waits for them, and re-layouts, per_device(): kv_rows = jnp.concatenate([key_rows, value_rows], axis=-1).transpose(0, 2...  5 us
    dot_general x1, matrix products, per_device(): jnp.dot(tokens_flat, key_weight, preferred_element_type=jnp.float32)  4.51 us
  transfers between devices with their start and end apart: 2, of which 1 were waited for; matrix products, arithmetic and copies ran while one was open for 8% of the time, Pallas kernels for 0%

commit v1 on v0

v1 whole, which is shorter than its diff:
```python
import functools

import jax
import jax.numpy as jnp
from jax import lax
from jax.experimental import pallas as pl
from jax.experimental.pallas import tpu as pltpu
from jax.sharding import PartitionSpec as P

HD = 64
KVH = 6
GROUP = 5
EPS_NORM = 0.0001
MESH = pl.DeviceIdType.MESH

NZ = 8
NX = 4
NSP = NZ * NX
NTP = 8
PAIRS = 3
ROWS = 64
LANES = 2 * HD
G8 = 8
R = PAIRS * G8
PLANE = NX * ROWS


def plane_offset(k):
    return jnp.where(k % 2 == 1, (k + 1) // 2, (NZ - k // 2) % NZ)


def split3(value):
    high = value.astype(jnp.bfloat16)
    rest = value - high.astype(jnp.float32)
    mid = rest.astype(jnp.bfloat16)
    low = (rest - mid.astype(jnp.float32)).astype(jnp.bfloat16)
    return high, mid, low


def exact_dot(value, ones):
    return sum(
        jnp.dot(part, ones, preferred_element_type=jnp.float32) for part in split3(value)
    )


def main_kernel(
    x_hbm, wk_hbm, wv_hbm, q_hbm, bias_hbm, land, usum,
    x_v, wk_v, wv_v, q_v, qp, bias_s, stage, vals, tots, part,
    x_sem, in_sem, send_sem, recv_sem, tot_in, part_in,
    tsend, trecv, psend, precv,
):
    sp = lax.axis_index("sp")
    tp = lax.axis_index("tp")
    z = sp // NX
    xm = sp % NX

    barrier = pltpu.get_barrier_semaphore()

    def greet_sp(i, c):
        pl.semaphore_signal(
            barrier, 1, device_id={"sp": (sp + i) % NSP}, device_id_type=MESH
        )
        return c

    lax.fori_loop(1, NSP, greet_sp, 0)
    for i in range(1, NTP):
        pl.semaphore_signal(
            barrier, 1, device_id={"tp": (tp + i) % NTP}, device_id_type=MESH
        )

    def x_copy(k):
        zt = (z + plane_offset(k)) % NZ
        return pltpu.make_async_copy(x_hbm.at[pl.ds(2 * zt, 2)], x_v.at[k], x_sem.at[k])

    wk_copy = pltpu.make_async_copy(wk_hbm, wk_v, in_sem.at[0])
    wv_copy = pltpu.make_async_copy(wv_hbm, wv_v, in_sem.at[1])
    q_copy = pltpu.make_async_copy(q_hbm, q_v, in_sem.at[2])
    bias_copy = pltpu.make_async_copy(bias_hbm, bias_s, in_sem.at[3])
    wk_copy.start()
    x_copy(0).start()
    wv_copy.start()
    for k in range(1, NZ):
        x_copy(k).start()
    q_copy.start()
    bias_copy.start()

    def block_copy(k, xt):
        zt = (z + plane_offset(k)) % NZ
        return pltpu.make_async_remote_copy(
            src_ref=stage.at[k, xt],
            dst_ref=land.at[:, sp],
            send_sem=send_sem.at[k, xt],
            recv_sem=recv_sem.at[k, xm],
            device_id={"sp": zt * NX + xt},
            device_id_type=MESH,
        )

    wk_copy.wait()
    wv_copy.wait()
    lane = lax.broadcasted_iota(jnp.int32, (ROWS, LANES), 1)
    low_half = lane < HD

    def project(k, c):
        x_copy(k).wait()
        x = x_v[k].reshape(2 * ROWS, x_v.shape[-1])
        keys = jnp.dot(x, wk_v[...], preferred_element_type=jnp.float32)
        values = jnp.dot(x, wv_v[...], preferred_element_type=jnp.float32)
        for half in range(2):
            for pair in range(3):
                kk = keys[half * ROWS : (half + 1) * ROWS, pair * LANES : (pair + 1) * LANES]
                vv = values[half * ROWS : (half + 1) * ROWS, pair * LANES : (pair + 1) * LANES]
                even = jnp.where(low_half, kk, pltpu.roll(vv, HD, 1))
                odd = jnp.where(low_half, pltpu.roll(kk, HD, 1), vv)
                for side, rows in ((0, even), (1, odd)):
                    head = 2 * pair + side
                    stage[k, 2 * half + head // 3, head % 3] = rows.astype(jnp.bfloat16)

        @pl.when(k == 0)
        def _():
            pl.semaphore_wait(barrier, NSP - 1 + NTP - 1)

        for xt in range(NX):
            @pl.when(jnp.logical_or(k > 0, xt != xm))
            def _():
                block_copy(k, xt).start()

        return c

    lax.fori_loop(0, NZ, project, 0)

    q_copy.wait()
    bias_copy.wait()
    qp[...] = jnp.zeros_like(qp)
    for p in range(PAIRS):
        for g in range(GROUP):
            qp[p, g : g + 1, 0:HD] = q_v[g, p : p + 1, :]
    row = lax.broadcasted_iota(jnp.int32, (R, PLANE), 0)
    bias = jnp.zeros((R, PLANE), jnp.float32)
    for p in range(PAIRS):
        head = (sp * PAIRS + p) % KVH
        for g in range(GROUP):
            bias = jnp.where(row == p * G8 + g, bias_s[head, g], bias)

    for xt in range(NX):
        @pl.when(xt == xm)
        def _():
            land[:, sp] = stage[0, xt]

    pos_i = lax.broadcasted_iota(jnp.int32, (PLANE, PLANE), 0)
    pos_j = lax.broadcasted_iota(jnp.int32, (PLANE, PLANE), 1)
    later = jnp.logical_and(pos_i > pos_j, pos_i // ROWS == pos_j // ROWS)
    later = jnp.where(later, 1.0, 0.0).astype(jnp.bfloat16)
    blk_i = lax.broadcasted_iota(jnp.int32, (PLANE, LANES), 0) // ROWS
    blk_j = lax.broadcasted_iota(jnp.int32, (PLANE, LANES), 1)
    lane_blk = lax.broadcasted_iota(jnp.int32, (G8, PLANE), 1) // ROWS

    def read_plane(k, total):
        zs = (z - plane_offset(k) + NZ) % NZ
        for xs in range(NX):
            @pl.when(jnp.logical_or(k > 0, xs != xm))
            def _():
                pltpu.make_async_remote_copy(
                    src_ref=stage.at[k, xs],
                    dst_ref=land.at[:, zs * NX + xs],
                    send_sem=send_sem.at[k, xs],
                    recv_sem=recv_sem.at[k, xs],
                    device_id={"sp": zs * NX + xs},
                    device_id_type=MESH,
                ).wait_recv()
        rows = [land[p, pl.ds(zs * NX, NX)].reshape(PLANE, LANES) for p in range(PAIRS)]
        scores = jnp.concatenate(
            [
                lax.dot_general(
                    qp[p], rows[p], (((1,), (1,)), ((), ())), preferred_element_type=jnp.float32
                )[:G8]
                for p in range(PAIRS)
            ],
            axis=0,
        )
        scores = scores * (1.0 / 8.0) + bias
        keep = -(jnp.maximum(scores, 0.0) + jnp.log1p(jnp.exp(-jnp.abs(scores))))
        inside = exact_dot(keep, later)
        pick = jnp.where(blk_i + zs * NX == blk_j, 1.0, 0.0).astype(jnp.bfloat16)
        total = total + exact_dot(keep, pick)
        weights = jnp.exp(scores + keep + inside)
        for p in range(PAIRS):
            w = weights[p * G8 : (p + 1) * G8]
            spread = jnp.concatenate(
                [jnp.where(lane_blk == b, w, 0.0) for b in range(NX)], axis=0
            ).astype(jnp.bfloat16)
            out = jnp.dot(spread, rows[p], preferred_element_type=jnp.float32)
            for b in range(NX):
                vals[zs * NX + b, p * G8 : (p + 1) * G8, :] = out[b * G8 : (b + 1) * G8]
        return total

    total = lax.fori_loop(0, NZ, read_plane, jnp.zeros((R, LANES), jnp.float32))

    def exchange(src, dst, ssem, rsem):
        for i in range(1, NTP):
            pltpu.make_async_remote_copy(
                src_ref=src, dst_ref=dst.at[i], send_sem=ssem.at[i], recv_sem=rsem.at[i],
                device_id={"tp": (tp + i) % NTP}, device_id_type=MESH,
            ).start()

    def arrived(src, dst, ssem, rsem):
        for i in range(1, NTP):
            pltpu.make_async_remote_copy(
                src_ref=src, dst_ref=dst.at[i], send_sem=ssem.at[i], recv_sem=rsem.at[i],
                device_id={"tp": (tp + i) % NTP}, device_id_type=MESH,
            ).wait()

    tots[...] = total
    exchange(tots, tot_in, tsend, trecv)
    arrived(tots, tot_in, tsend, trecv)
    every = total
    inside_later = jnp.zeros_like(total)
    for i in range(1, NTP):
        other = tot_in[i]
        every = every + other
        inside_later = inside_later + jnp.where(tp - i < 0, other, 0.0)
    chunk_i = lax.broadcasted_iota(jnp.int32, (LANES, LANES), 0)
    chunk_j = lax.broadcasted_iota(jnp.int32, (LANES, LANES), 1)
    after = jnp.where(chunk_i > chunk_j, 1.0, 0.0).astype(jnp.bfloat16)
    scale = jnp.exp(exact_dot(every, after) + inside_later)
    partial = jnp.zeros((R, LANES), jnp.float32)
    for b in range(NSP):
        partial = partial + scale[:, b : b + 1] * vals[b]
    part[...] = partial
    exchange(part, part_in, psend, precv)

    def drain(k, c):
        for xt in range(NX):
            @pl.when(jnp.logical_or(k > 0, xt != xm))
            def _():
                block_copy(k, xt).wait_send()
        return c

    lax.fori_loop(0, NZ, drain, 0)
    arrived(part, part_in, psend, precv)
    for i in range(1, NTP):
        partial = partial + part_in[i]
    usum[...] = partial


def finish_kernel(land, usum, stored, first_read, fr_v, out_sem):
    copy = pltpu.make_async_copy(land, stored, out_sem.at[0])
    copy.start()
    summed = usum[...]
    lane = lax.broadcasted_iota(jnp.int32, (R, LANES), 1)
    summed = jnp.where(lane >= HD, summed, 0.0)
    squares = jnp.sum(summed * summed, axis=-1, keepdims=True) * (1.0 / HD)
    normed = summed * lax.rsqrt(squares + EPS_NORM)
    swapped = pltpu.roll(normed, HD, 1)
    for p in range(PAIRS):
        for g in range(GROUP):
            source = normed if g % 2 else swapped
            lo = (g % 2) * HD
            fr_v[p : p + 1, g * HD : (g + 1) * HD] = source[
                p * G8 + g : p * G8 + g + 1, lo : lo + HD
            ]
    first_read[...] = fr_v[...].astype(jnp.bfloat16)
    copy.wait()


def per_device(layer_input, key_weight, value_weight, queries, head_bias):
    width = layer_input.shape[-1]
    hbm = pl.BlockSpec(memory_space=pltpu.HBM)
    vmem = pl.BlockSpec(memory_space=pltpu.VMEM)
    land, usum = pl.pallas_call(
        main_kernel,
        out_shape=(
            jax.ShapeDtypeStruct((PAIRS, NSP, ROWS, LANES), jnp.bfloat16),
            jax.ShapeDtypeStruct((R, LANES), jnp.float32),
        ),
        in_specs=[hbm] * 5,
        out_specs=(vmem, vmem),
        scratch_shapes=[
            pltpu.VMEM((NZ, 2, ROWS, width), jnp.bfloat16),
            pltpu.VMEM(key_weight.shape, jnp.bfloat16),
            pltpu.VMEM(value_weight.shape, jnp.bfloat16),
            pltpu.VMEM((GROUP, PAIRS, HD), jnp.bfloat16),
            pltpu.VMEM((PAIRS, 16, LANES), jnp.bfloat16),
            pltpu.SMEM(head_bias.shape, jnp.float32),
            pltpu.VMEM((NZ, NX, PAIRS, ROWS, LANES), jnp.bfloat16),
            pltpu.VMEM((NSP, R, LANES), jnp.float32),
            pltpu.VMEM((R, LANES), jnp.float32),
            pltpu.VMEM((R, LANES), jnp.float32),
            pltpu.SemaphoreType.DMA((NZ,)),
            pltpu.SemaphoreType.DMA((4,)),
            pltpu.SemaphoreType.DMA((NZ, NX)),
            pltpu.SemaphoreType.DMA((NZ, NX)),
            pltpu.VMEM((NTP, R, LANES), jnp.float32),
            pltpu.VMEM((NTP, R, LANES), jnp.float32),
            pltpu.SemaphoreType.DMA((NTP,)),
            pltpu.SemaphoreType.DMA((NTP,)),
            pltpu.SemaphoreType.DMA((NTP,)),
            pltpu.SemaphoreType.DMA((NTP,)),
        ],
        compiler_params=pltpu.CompilerParams(
            collective_id=0, has_side_effects=True, vmem_limit_bytes=53672 * 1024
        ),
        name="project_exchange_read",
    )(layer_input, key_weight, value_weight, queries.transpose(1, 0, 2), head_bias)
    stored, first_read = pl.pallas_call(
        finish_kernel,
        out_shape=(
            jax.ShapeDtypeStruct(land.shape, jnp.bfloat16),
            jax.ShapeDtypeStruct((PAIRS, GROUP * HD), jnp.bfloat16),
        ),
        in_specs=[pl.BlockSpec(memory_space=pl.ANY), vmem],
        out_specs=(pl.BlockSpec(memory_space=pl.ANY), vmem),
        scratch_shapes=[
            pltpu.VMEM((PAIRS, GROUP * HD), jnp.float32),
            pltpu.SemaphoreType.DMA((1,)),
        ],
        compiler_params=pltpu.CompilerParams(vmem_limit_bytes=8 * 1024 * 1024),
        name="finish",
    )(land, usum)
    return stored, first_read


def solution(mesh):
    in_specs = (P(None, ("sp", "tp"), None), P(), P(), P("sp", None, None), P())
    out_specs = (P("sp", None, "tp", None), P("sp", None))
    return jax.shard_map(
        per_device, mesh=mesh, in_specs=in_specs, out_specs=out_specs, check_vma=False
    )
```

time: 117 us -> 61.8 us (0.53)
  the two profiles are of different devices: /device:TPU:1 before, /device:TPU:39 now
where the time goes in v1:
time: 61.8 us; the launch traced here: 61.6 us
  Pallas kernels  59.6 us (96%)
  local copies, waits for them, and re-layouts  1.37 us (2%)
  between operations  0.65 us (1%)
    pallas_call x1, Pallas kernels, per_device(): pl.pallas_call(main_kernel, out_shape=(jax.ShapeDtypeStruct((PAIRS, NSP,...  57.9 us
    pallas_call x1, Pallas kernels, per_device(): pl.pallas_call(finish_kernel, out_shape=(jax.ShapeDtypeStruct(land.shape,...  1.73 us
    unnamed x4, local copies, waits for them, and re-layouts  1.37 us

profile of v1, /device:TPU:39, one launch (start us, length us, event | category | flops | bytes accessed | tf_op | source)
XLA Modules:
  0.0 61.6 jit_solution(6905918474822475412)
XLA Ops:
  0.6 0.0 copy-start
  0.6 0.7 %copy-done = bf16[3,5,64]{2,0,1:T(4,128)(2,1)S(1)} copy-done((bf16[3,5,64]{2,0,1:T(4,128)(2,1)S(1)}, bf16[3,5,64]{2,0,1:T(4,128)(2,1)}, u32[]{:S(2)}) %copy-start) | copy-done | bytes 1944
  1.3 0.0 copy-start.1
  1.3 0.7 %copy-done.1 = f32[6,5]{1,0:T(8,128)S(1)} copy-done((f32[6,5]{1,0:T(8,128)S(1)}, f32[6,5]{1,0:T(8,128)}, u32[]{:S(2)}) %copy-start.1) | copy-done | bytes 144
  2.0 57.9 %project_exchange_read.1 = (bf16[3,32,64,128]{3,2,1,0:T(8,128)(2,1)S(1)}, f32[24,128]{1,0:T(8,128)S(1)}) custom-call(bf16[16,64,2048]{2,1,0:T(8,128)(2,1)} %x_hbm.1, bf16[2048,384]{1,0:T(8,128)(2,1)} %wk_hbm.1, bf16[2048,384]{1,0:T(8,128)(2,1)} %wv_hbm.1, bf16[5,3,64]{2,1,0:T(4,128)(2,1)S(1)} %bitcast.1, f32[6,5]{1,0:T(8,128)S(1)} %copy-done.1), custom_call_target="tpu_custom_call" | custom-call | tf_op jit(solution)/shard_map/project_exchange_read/pallas_call | solution.py:269
  59.9 1.7 %finish.1 = (bf16[3,32,64,128]{3,2,1,0:T(8,128)(2,1)}, bf16[3,320]{1,0:T(4,128)(2,1)}) custom-call(bf16[3,32,64,128]{3,2,1,0:T(8,128)(2,1)S(1)} %get-tuple-element.4.land, f32[24,128]{1,0:T(8,128)S(1)} %get-tuple-element.5.usum), custom_call_target="tpu_custom_call" | custom-call | tf_op jit(solution)/shard_map/finish/pallas_call | solution.py:304
Async XLA Ops:
  0.6 0.7 %copy-start = (bf16[3,5,64]{2,0,1:T(4,128)(2,1)S(1)}, bf16[3,5,64]{2,0,1:T(4,128)(2,1)}, u32[]{:S(2)}) copy-start(bf16[3,5,64]{2,0,1:T(4,128)(2,1)} %param.8) | copy-start | bytes 5764
  1.3 0.7 %copy-start.1 = (f32[6,5]{1,0:T(8,128)S(1)}, f32[6,5]{1,0:T(8,128)}, u32[]{:S(2)}) copy-start(f32[6,5]{1,0:T(8,128)} %bias_hbm.1) | copy-start | bytes 364

commit v2 on v1

--- a/solution.py
+++ b/solution.py
@@ -20,13 +20,19 @@
 PAIRS = 3
 ROWS = 64
 LANES = 2 * HD
-G8 = 8
-R = PAIRS * G8
+R = 16
 PLANE = NX * ROWS
+ORDER = (1, 7, 0, 2, 6, 3, 5, 4)
+OWN = ORDER.index(0)
+LAST = NZ - 1
+FIRST_READS = 3
 
 
 def plane_offset(k):
-    return jnp.where(k % 2 == 1, (k + 1) // 2, (NZ - k // 2) % NZ)
+    offset = ORDER[-1]
+    for at, value in enumerate(ORDER[:-1]):
+        offset = jnp.where(k == at, value, offset)
+    return offset
 
 
 def split3(value):
@@ -45,9 +51,10 @@
 
 def main_kernel(
     x_hbm, wk_hbm, wv_hbm, q_hbm, bias_hbm, land, usum,
-    x_v, wk_v, wv_v, q_v, qp, bias_s, stage, vals, tots, part,
-    x_sem, in_sem, send_sem, recv_sem, tot_in, part_in,
-    tsend, trecv, psend, precv,
+    x_v, wk_v, wv_v, q_v, qc, bias_s, stage, vals, tots, part, tot_in, part_in,
+    q_in, tv_out, tv_in,
+    x_sem, in_sem, send_sem, recv_sem, tsend, trecv, psend, precv,
+    qsend, qrecv, vsend, vrecv,
 ):
     sp = lax.axis_index("sp")
     tp = lax.axis_index("tp")
@@ -55,14 +62,10 @@
     xm = sp % NX
 
     barrier = pltpu.get_barrier_semaphore()
-
-    def greet_sp(i, c):
+    for i in range(1, NSP):
         pl.semaphore_signal(
             barrier, 1, device_id={"sp": (sp + i) % NSP}, device_id_type=MESH
         )
-        return c
-
-    lax.fori_loop(1, NSP, greet_sp, 0)
     for i in range(1, NTP):
         pl.semaphore_signal(
             barrier, 1, device_id={"tp": (tp + i) % NTP}, device_id_type=MESH
@@ -95,10 +98,99 @@
             device_id_type=MESH,
         )
 
+    def send_plane(k):
+        for dx in (1, 3, 2, 0):
+            @pl.when(jnp.logical_or(k != OWN, dx != 0))
+            def _():
+                block_copy(k, (xm + dx) % NX).start()
+
+    row_pair = lax.broadcasted_iota(jnp.int32, (R, PLANE), 0) // GROUP
+    row_pair_v = lax.broadcasted_iota(jnp.int32, (NX * R, LANES), 0) % R // GROUP
+    lane_blk = lax.broadcasted_iota(jnp.int32, (R, PLANE), 1) // ROWS
+    pos_i = lax.broadcasted_iota(jnp.int32, (PLANE, PLANE), 0)
+    pos_j = lax.broadcasted_iota(jnp.int32, (PLANE, PLANE), 1)
+    later = jnp.logical_and(pos_i > pos_j, pos_i // ROWS == pos_j // ROWS)
+    later = jnp.where(later, 1.0, 0.0).astype(jnp.bfloat16)
+    blk_i = lax.broadcasted_iota(jnp.int32, (PLANE, LANES), 0) // ROWS
+    blk_j = lax.broadcasted_iota(jnp.int32, (PLANE, LANES), 1)
+    lane = lax.broadcasted_iota(jnp.int32, (R, LANES), 1)
+
+    def bias_table(odd):
+        row = lax.broadcasted_iota(jnp.int32, (R, PLANE), 0)
+        table = jnp.zeros((R, PLANE), jnp.float32)
+        for p in range(PAIRS):
+            for g in range(GROUP):
+                value = jnp.where(odd, bias_s[PAIRS + p, g], bias_s[p, g])
+                table = jnp.where(row == p * GROUP + g, value, table)
+        return table
+
+    def read(rows, query, bias, first):
+        scores = jnp.zeros((R, PLANE), jnp.float32)
+        for p in range(PAIRS):
+            dots = lax.dot_general(
+                query, rows[p], (((1,), (1,)), ((), ())), preferred_element_type=jnp.float32
+            )
+            if dots.shape[0] == R:
+                scores = jnp.where(row_pair == p, dots, scores)
+            else:
+                for b in range(NX):
+                    mine = jnp.logical_and(row_pair == p, lane_blk == b)
+                    scores = jnp.where(mine, dots[b * R : (b + 1) * R], scores)
+        scores = scores * (1.0 / 8.0) + bias
+        keep = -(jnp.maximum(scores, 0.0) + jnp.log1p(jnp.exp(-jnp.abs(scores))))
+        inside = exact_dot(keep, later)
+        pick = jnp.where(blk_i + first == blk_j, 1.0, 0.0).astype(jnp.bfloat16)
+        totals = exact_dot(keep, pick)
+        weights = jnp.exp(scores + keep + inside)
+        spread = jnp.concatenate(
+            [jnp.where(lane_blk == b, weights, 0.0) for b in range(NX)], axis=0
+        ).astype(jnp.bfloat16)
+        values = jnp.zeros((NX * R, LANES), jnp.float32)
+        for p in range(PAIRS):
+            out = jnp.dot(spread, rows[p], preferred_element_type=jnp.float32)
+            values = jnp.where(row_pair_v == p, out, values)
+        return totals, values
+
+    q_copy.wait()
+    bias_copy.wait()
+    qc[...] = jnp.zeros_like(qc)
+    for p in range(PAIRS):
+        for g in range(GROUP):
+            qc[p * GROUP + g : p * GROUP + g + 1, 0:HD] = q_v[g, p : p + 1, :]
+
+    far = (z + NZ // 2) % NZ
+
+    def query_copy(xt, slot):
+        return pltpu.make_async_remote_copy(
+            src_ref=qc, dst_ref=q_in.at[slot], send_sem=qsend.at[xt], recv_sem=qrecv.at[slot],
+            device_id={"sp": far * NX + xt}, device_id_type=MESH,
+        )
+
+    def read_copy(xt, slot):
+        return pltpu.make_async_remote_copy(
+            src_ref=tv_out.at[xt], dst_ref=tv_in.at[slot],
+            send_sem=vsend.at[xt], recv_sem=vrecv.at[slot],
+            device_id={"sp": far * NX + xt}, device_id_type=MESH,
+        )
+
+    def read_at_source():
+        for xt in range(NX):
+            query_copy(xt, xt).wait_recv()
+        rows = [stage[LAST, :, p].reshape(PLANE, LANES) for p in range(PAIRS)]
+        totals, values = read(
+            rows, q_in[...].reshape(NX * R, LANES), bias_table(lane_blk % 2 == 1), 0
+        )
+        for xt in range(NX):
+            message = values[xt * R : (xt + 1) * R]
+            for at, piece in enumerate(split3(totals[:, xt : xt + 1])):
+                message = jnp.where(lane == at, piece.astype(jnp.float32), message)
+            tv_out[xt] = message.astype(jnp.bfloat16)
+        for dx in (1, 3, 2, 0):
+            read_copy((xm + dx) % NX, xm).start()
+
     wk_copy.wait()
     wv_copy.wait()
-    lane = lax.broadcasted_iota(jnp.int32, (ROWS, LANES), 1)
-    low_half = lane < HD
+    low_half = lax.broadcasted_iota(jnp.int32, (ROWS, LANES), 1) < HD
 
     def project(k, c):
         x_copy(k).wait()
@@ -118,100 +210,74 @@
         @pl.when(k == 0)
         def _():
             pl.semaphore_wait(barrier, NSP - 1 + NTP - 1)
-
-        for xt in range(NX):
-            @pl.when(jnp.logical_or(k > 0, xt != xm))
-            def _():
-                block_copy(k, xt).start()
+            for dx in range(NX):
+                query_copy((xm + dx) % NX, xm).start()
+
+        @pl.when(k != LAST)
+        def _():
+            send_plane(k)
 
         return c
 
     lax.fori_loop(0, NZ, project, 0)
-
-    q_copy.wait()
-    bias_copy.wait()
-    qp[...] = jnp.zeros_like(qp)
-    for p in range(PAIRS):
-        for g in range(GROUP):
-            qp[p, g : g + 1, 0:HD] = q_v[g, p : p + 1, :]
-    row = lax.broadcasted_iota(jnp.int32, (R, PLANE), 0)
-    bias = jnp.zeros((R, PLANE), jnp.float32)
-    for p in range(PAIRS):
-        head = (sp * PAIRS + p) % KVH
-        for g in range(GROUP):
-            bias = jnp.where(row == p * G8 + g, bias_s[head, g], bias)
 
     for xt in range(NX):
         @pl.when(xt == xm)
         def _():
-            land[:, sp] = stage[0, xt]
-
-    pos_i = lax.broadcasted_iota(jnp.int32, (PLANE, PLANE), 0)
-    pos_j = lax.broadcasted_iota(jnp.int32, (PLANE, PLANE), 1)
-    later = jnp.logical_and(pos_i > pos_j, pos_i // ROWS == pos_j // ROWS)
-    later = jnp.where(later, 1.0, 0.0).astype(jnp.bfloat16)
-    blk_i = lax.broadcasted_iota(jnp.int32, (PLANE, LANES), 0) // ROWS
-    blk_j = lax.broadcasted_iota(jnp.int32, (PLANE, LANES), 1)
-    lane_blk = lax.broadcasted_iota(jnp.int32, (G8, PLANE), 1) // ROWS
+            land[:, sp] = stage[OWN, xt]
+
+    own_bias = bias_table(sp % 2 == 1)
+
+    def arrival(k, xs):
+        zs = (z - plane_offset(k) + NZ) % NZ
+        return pltpu.make_async_remote_copy(
+            src_ref=stage.at[k, xs],
+            dst_ref=land.at[:, zs * NX + xs],
+            send_sem=send_sem.at[k, xs],
+            recv_sem=recv_sem.at[k, xs],
+            device_id={"sp": zs * NX + xs},
+            device_id_type=MESH,
+        )
 
     def read_plane(k, total):
         zs = (z - plane_offset(k) + NZ) % NZ
         for xs in range(NX):
-            @pl.when(jnp.logical_or(k > 0, xs != xm))
+            @pl.when(jnp.logical_or(k != OWN, xs != xm))
             def _():
-                pltpu.make_async_remote_copy(
-                    src_ref=stage.at[k, xs],
-                    dst_ref=land.at[:, zs * NX + xs],
-                    send_sem=send_sem.at[k, xs],
-                    recv_sem=recv_sem.at[k, xs],
-                    device_id={"sp": zs * NX + xs},
-                    device_id_type=MESH,
-                ).wait_recv()
+                arrival(k, xs).wait_recv()
         rows = [land[p, pl.ds(zs * NX, NX)].reshape(PLANE, LANES) for p in range(PAIRS)]
-        scores = jnp.concatenate(
-            [
-                lax.dot_general(
-                    qp[p], rows[p], (((1,), (1,)), ((), ())), preferred_element_type=jnp.float32
-                )[:G8]
-                for p in range(PAIRS)
-            ],
-            axis=0,
-        )
-        scores = scores * (1.0 / 8.0) + bias
-        keep = -(jnp.maximum(scores, 0.0) + jnp.log1p(jnp.exp(-jnp.abs(scores))))
-        inside = exact_dot(keep, later)
-        pick = jnp.where(blk_i + zs * NX == blk_j, 1.0, 0.0).astype(jnp.bfloat16)
-        total = total + exact_dot(keep, pick)
-        weights = jnp.exp(scores + keep + inside)
-        for p in range(PAIRS):
-            w = weights[p * G8 : (p + 1) * G8]
-            spread = jnp.concatenate(
-                [jnp.where(lane_blk == b, w, 0.0) for b in range(NX)], axis=0
-            ).astype(jnp.bfloat16)
-            out = jnp.dot(spread, rows[p], preferred_element_type=jnp.float32)
-            for b in range(NX):
-                vals[zs * NX + b, p * G8 : (p + 1) * G8, :] = out[b * G8 : (b + 1) * G8]
-        return total
-
-    total = lax.fori_loop(0, NZ, read_plane, jnp.zeros((R, LANES), jnp.float32))
+        totals, values = read(rows, qc[...], own_bias, zs * NX)
+        for b in range(NX):
+            vals[zs * NX + b] = values[b * R : (b + 1) * R]
+        return total + totals
+
+    total = jnp.zeros((R, LANES), jnp.float32)
+    total = lax.fori_loop(0, FIRST_READS, read_plane, total)
+    read_at_source()
+    send_plane(LAST)
+    total = lax.fori_loop(FIRST_READS, LAST, read_plane, total)
+    for xs in range(NX):
+        read_copy(xs, xs).wait_recv()
+        message = tv_in[xs].astype(jnp.float32)
+        sums = message[:, 0:1] + message[:, 1:2] + message[:, 2:3]
+        total = total + jnp.where(lane == far * NX + xs, sums, 0.0)
+        vals[far * NX + xs] = message
 
     def exchange(src, dst, ssem, rsem):
-        for i in range(1, NTP):
+        return [
             pltpu.make_async_remote_copy(
                 src_ref=src, dst_ref=dst.at[i], send_sem=ssem.at[i], recv_sem=rsem.at[i],
                 device_id={"tp": (tp + i) % NTP}, device_id_type=MESH,
-            ).start()
-
-    def arrived(src, dst, ssem, rsem):
-        for i in range(1, NTP):
-            pltpu.make_async_remote_copy(
-                src_ref=src, dst_ref=dst.at[i], send_sem=ssem.at[i], recv_sem=rsem.at[i],
-                device_id={"tp": (tp + i) % NTP}, device_id_type=MESH,
-            ).wait()
+            )
+            for i in range(1, NTP)
+        ]
 
     tots[...] = total
-    exchange(tots, tot_in, tsend, trecv)
-    arrived(tots, tot_in, tsend, trecv)
+    copies = exchange(tots, tot_in, tsend, trecv)
+    for copy in copies:
+        copy.start()
+    for copy in copies:
+        copy.wait()
     every = total
     inside_later = jnp.zeros_like(total)
     for i in range(1, NTP):
@@ -226,20 +292,29 @@
     for b in range(NSP):
         partial = partial + scale[:, b : b + 1] * vals[b]
     part[...] = partial
-    exchange(part, part_in, psend, precv)
+    copies = exchange(part, part_in, psend, precv)
+    for copy in copies:
+        copy.start()
+    for copy in copies:
+        copy.wait()
+    for i in range(1, NTP):
+        partial = partial + part_in[i]
+    usum[...] = partial
+
+    for xs in range(NX):
+        arrival(LAST, xs).wait_recv()
 
     def drain(k, c):
         for xt in range(NX):
-            @pl.when(jnp.logical_or(k > 0, xt != xm))
+            @pl.when(jnp.logical_or(k != OWN, xt != xm))
             def _():
                 block_copy(k, xt).wait_send()
         return c
 
     lax.fori_loop(0, NZ, drain, 0)
-    arrived(part, part_in, psend, precv)
-    for i in range(1, NTP):
-        partial = partial + part_in[i]
-    usum[...] = partial
+    for xt in range(NX):
+        query_copy(xt, xt).wait_send()
+        read_copy(xt, xt).wait_send()
 
 
 def finish_kernel(land, usum, stored, first_read, fr_v, out_sem):
@@ -256,7 +331,7 @@
             source = normed if g % 2 else swapped
             lo = (g % 2) * HD
             fr_v[p : p + 1, g * HD : (g + 1) * HD] = source[
-                p * G8 + g : p * G8 + g + 1, lo : lo + HD
+                p * GROUP + g : p * GROUP + g + 1, lo : lo + HD
             ]
     first_read[...] = fr_v[...].astype(jnp.bfloat16)
     copy.wait()
@@ -279,22 +354,29 @@
             pltpu.VMEM(key_weight.shape, jnp.bfloat16),
             pltpu.VMEM(value_weight.shape, jnp.bfloat16),
             pltpu.VMEM((GROUP, PAIRS, HD), jnp.bfloat16),
-            pltpu.VMEM((PAIRS, 16, LANES), jnp.bfloat16),
+            pltpu.VMEM((R, LANES), jnp.bfloat16),
             pltpu.SMEM(head_bias.shape, jnp.float32),
             pltpu.VMEM((NZ, NX, PAIRS, ROWS, LANES), jnp.bfloat16),
             pltpu.VMEM((NSP, R, LANES), jnp.float32),
             pltpu.VMEM((R, LANES), jnp.float32),
             pltpu.VMEM((R, LANES), jnp.float32),
+            pltpu.VMEM((NTP, R, LANES), jnp.float32),
+            pltpu.VMEM((NTP, R, LANES), jnp.float32),
+            pltpu.VMEM((NX, R, LANES), jnp.bfloat16),
+            pltpu.VMEM((NX, R, LANES), jnp.bfloat16),
+            pltpu.VMEM((NX, R, LANES), jnp.bfloat16),
             pltpu.SemaphoreType.DMA((NZ,)),
             pltpu.SemaphoreType.DMA((4,)),
             pltpu.SemaphoreType.DMA((NZ, NX)),
             pltpu.SemaphoreType.DMA((NZ, NX)),
-            pltpu.VMEM((NTP, R, LANES), jnp.float32),
-            pltpu.VMEM((NTP, R, LANES), jnp.float32),
             pltpu.SemaphoreType.DMA((NTP,)),
             pltpu.SemaphoreType.DMA((NTP,)),
             pltpu.SemaphoreType.DMA((NTP,)),
             pltpu.SemaphoreType.DMA((NTP,)),
+            pltpu.SemaphoreType.DMA((NX,)),
+            pltpu.SemaphoreType.DMA((NX,)),
+            pltpu.SemaphoreType.DMA((NX,)),
+            pltpu.SemaphoreType.DMA((NX,)),
         ],
         compiler_params=pltpu.CompilerParams(
             collective_id=0, has_side_effects=True, vmem_limit_bytes=53672 * 1024

time: 61.8 us -> 57 us (0.922)
  the two profiles are of different devices: /device:TPU:39 before, /device:TPU:1 now
where the time goes in v2:
time: 57 us; the launch traced here: 56.9 us
  Pallas kernels  54.8 us (96%)
  local copies, waits for them, and re-layouts  1.37 us (2%)
  between operations  0.65 us (1%)
    pallas_call x1, Pallas kernels, per_device(): pl.pallas_call(main_kernel, out_shape=(jax.ShapeDtypeStruct((PAIRS, NSP,...  53.1 us
    pallas_call x1, Pallas kernels, per_device(): pl.pallas_call(finish_kernel, out_shape=(jax.ShapeDtypeStruct(land.shape,...  1.73 us
    unnamed x4, local copies, waits for them, and re-layouts  1.37 us

profile of v2, /device:TPU:1, one launch (start us, length us, event | category | flops | bytes accessed | tf_op | source)
XLA Modules:
  0.0 56.9 jit_solution(11857909678957838046)
XLA Ops:
  0.6 0.0 copy-start
  0.6 0.7 %copy-done = bf16[3,5,64]{2,0,1:T(4,128)(2,1)S(1)} copy-done((bf16[3,5,64]{2,0,1:T(4,128)(2,1)S(1)}, bf16[3,5,64]{2,0,1:T(4,128)(2,1)}, u32[]{:S(2)}) %copy-start) | copy-done | bytes 1944
  1.3 0.0 copy-start.1
  1.3 0.7 %copy-done.1 = f32[6,5]{1,0:T(8,128)S(1)} copy-done((f32[6,5]{1,0:T(8,128)S(1)}, f32[6,5]{1,0:T(8,128)}, u32[]{:S(2)}) %copy-start.1) | copy-done | bytes 144
  2.0 53.1 %project_exchange_read.1 = (bf16[3,32,64,128]{3,2,1,0:T(8,128)(2,1)S(1)}, f32[16,128]{1,0:T(8,128)S(1)}) custom-call(bf16[16,64,2048]{2,1,0:T(8,128)(2,1)} %x_hbm.1, bf16[2048,384]{1,0:T(8,128)(2,1)} %wk_hbm.1, bf16[2048,384]{1,0:T(8,128)(2,1)} %wv_hbm.1, bf16[5,3,64]{2,1,0:T(4,128)(2,1)S(1)} %bitcast.1, f32[6,5]{1,0:T(8,128)S(1)} %copy-done.1), custom_call_target="tpu_custom_call" | custom-call | tf_op jit(solution)/shard_map/project_exchange_read/pallas_call | solution.py:344
  55.1 1.7 %finish.1 = (bf16[3,32,64,128]{3,2,1,0:T(8,128)(2,1)}, bf16[3,320]{1,0:T(4,128)(2,1)}) custom-call(bf16[3,32,64,128]{3,2,1,0:T(8,128)(2,1)S(1)} %get-tuple-element.4.land, f32[16,128]{1,0:T(8,128)S(1)} %get-tuple-element.5.usum), custom_call_target="tpu_custom_call" | custom-call | tf_op jit(solution)/shard_map/finish/pallas_call | solution.py:386
Async XLA Ops:
  0.6 0.7 %copy-start = (bf16[3,5,64]{2,0,1:T(4,128)(2,1)S(1)}, bf16[3,5,64]{2,0,1:T(4,128)(2,1)}, u32[]{:S(2)}) copy-start(bf16[3,5,64]{2,0,1:T(4,128)(2,1)} %param.8) | copy-start | bytes 5764
  1.3 0.7 %copy-start.1 = (f32[6,5]{1,0:T(8,128)S(1)}, f32[6,5]{1,0:T(8,128)}, u32[]{:S(2)}) copy-start(f32[6,5]{1,0:T(8,128)} %bias_hbm.1) | copy-start | bytes 364

commit v3 on v2

--- a/solution.py
+++ b/solution.py
@@ -22,10 +22,10 @@
 LANES = 2 * HD
 R = 16
 PLANE = NX * ROWS
-ORDER = (1, 7, 0, 2, 6, 3, 5, 4)
+CUTS = 4
+ORDER = (1, 7, 0, 2, 6, 4, 3, 5)
 OWN = ORDER.index(0)
-LAST = NZ - 1
-FIRST_READS = 3
+LAST = ORDER.index(NZ // 2)
 
 
 def plane_offset(k):
@@ -44,16 +44,17 @@
 
 
 def exact_dot(value, ones):
-    return sum(
-        jnp.dot(part, ones, preferred_element_type=jnp.float32) for part in split3(value)
-    )
+    rows = value.shape[0]
+    parts = jnp.concatenate(split3(value), axis=0)
+    sums = jnp.dot(parts, ones, preferred_element_type=jnp.float32)
+    return sums[:rows] + sums[rows : 2 * rows] + sums[2 * rows :]
 
 
 def main_kernel(
     x_hbm, wk_hbm, wv_hbm, q_hbm, bias_hbm, land, usum,
     x_v, wk_v, wv_v, q_v, qc, bias_s, stage, vals, tots, part, tot_in, part_in,
-    q_in, tv_out, tv_in,
-    x_sem, in_sem, send_sem, recv_sem, tsend, trecv, psend, precv,
+    q_out, q_in, tv_out, tv_in,
+    x_sem, w_sem, in_sem, send_sem, recv_sem, tsend, trecv, psend, precv,
     qsend, qrecv, vsend, vrecv,
 ):
     sp = lax.axis_index("sp")
@@ -61,6 +62,30 @@
     z = sp // NX
     xm = sp % NX
 
+    def x_copy(k):
+        zt = (z + plane_offset(k)) % NZ
+        return pltpu.make_async_copy(x_hbm.at[pl.ds(2 * zt, 2)], x_v.at[k], x_sem.at[k])
+
+    def weight_copies(w_hbm, w_v, first):
+        part = w_v.shape[0] // CUTS
+        return [
+            pltpu.make_async_copy(
+                w_hbm.at[pl.ds(i * part, part)], w_v.at[pl.ds(i * part, part)], w_sem.at[first + i]
+            )
+            for i in range(CUTS)
+        ]
+
+    weights = weight_copies(wk_hbm, wk_v, 0) + weight_copies(wv_hbm, wv_v, CUTS)
+    q_copy = pltpu.make_async_copy(q_hbm, q_v, in_sem.at[0])
+    bias_copy = pltpu.make_async_copy(bias_hbm, bias_s, in_sem.at[1])
+    x_copy(0).start()
+    for copy in weights:
+        copy.start()
+    q_copy.start()
+    bias_copy.start()
+    for k in range(1, NZ):
+        x_copy(k).start()
+
     barrier = pltpu.get_barrier_semaphore()
     for i in range(1, NSP):
         pl.semaphore_signal(
@@ -70,22 +95,6 @@
         pl.semaphore_signal(
             barrier, 1, device_id={"tp": (tp + i) % NTP}, device_id_type=MESH
         )
-
-    def x_copy(k):
-        zt = (z + plane_offset(k)) % NZ
-        return pltpu.make_async_copy(x_hbm.at[pl.ds(2 * zt, 2)], x_v.at[k], x_sem.at[k])
-
-    wk_copy = pltpu.make_async_copy(wk_hbm, wk_v, in_sem.at[0])
-    wv_copy = pltpu.make_async_copy(wv_hbm, wv_v, in_sem.at[1])
-    q_copy = pltpu.make_async_copy(q_hbm, q_v, in_sem.at[2])
-    bias_copy = pltpu.make_async_copy(bias_hbm, bias_s, in_sem.at[3])
-    wk_copy.start()
-    x_copy(0).start()
-    wv_copy.start()
-    for k in range(1, NZ):
-        x_copy(k).start()
-    q_copy.start()
-    bias_copy.start()
 
     def block_copy(k, xt):
         zt = (z + plane_offset(k)) % NZ
@@ -138,9 +147,9 @@
                     scores = jnp.where(mine, dots[b * R : (b + 1) * R], scores)
         scores = scores * (1.0 / 8.0) + bias
         keep = -(jnp.maximum(scores, 0.0) + jnp.log1p(jnp.exp(-jnp.abs(scores))))
-        inside = exact_dot(keep, later)
         pick = jnp.where(blk_i + first == blk_j, 1.0, 0.0).astype(jnp.bfloat16)
-        totals = exact_dot(keep, pick)
+        sums = exact_dot(keep, jnp.concatenate([later, pick], axis=1))
+        inside, totals = sums[:, :PLANE], sums[:, PLANE:]
         weights = jnp.exp(scores + keep + inside)
         spread = jnp.concatenate(
             [jnp.where(lane_blk == b, weights, 0.0) for b in range(NX)], axis=0
@@ -157,12 +166,14 @@
     for p in range(PAIRS):
         for g in range(GROUP):
             qc[p * GROUP + g : p * GROUP + g + 1, 0:HD] = q_v[g, p : p + 1, :]
+    wide = qc[...].astype(jnp.float32)
+    q_out[...] = (wide[: R // 2] + pltpu.roll(wide[R // 2 :], HD, 1)).astype(jnp.bfloat16)
 
     far = (z + NZ // 2) % NZ
 
     def query_copy(xt, slot):
         return pltpu.make_async_remote_copy(
-            src_ref=qc, dst_ref=q_in.at[slot], send_sem=qsend.at[xt], recv_sem=qrecv.at[slot],
+            src_ref=q_out, dst_ref=q_in.at[slot], send_sem=qsend.at[xt], recv_sem=qrecv.at[slot],
             device_id={"sp": far * NX + xt}, device_id_type=MESH,
         )
 
@@ -177,9 +188,13 @@
         for xt in range(NX):
             query_copy(xt, xt).wait_recv()
         rows = [stage[LAST, :, p].reshape(PLANE, LANES) for p in range(PAIRS)]
-        totals, values = read(
-            rows, q_in[...].reshape(NX * R, LANES), bias_table(lane_blk % 2 == 1), 0
-        )
+        low = lane[: R // 2] < HD
+        pieces = []
+        for xt in range(NX):
+            wide = q_in[xt].astype(jnp.float32)
+            pieces += [jnp.where(low, wide, 0.0), jnp.where(low, pltpu.roll(wide, HD, 1), 0.0)]
+        query = jnp.concatenate(pieces, axis=0).astype(jnp.bfloat16)
+        totals, values = read(rows, query, bias_table(lane_blk % 2 == 1), 0)
         for xt in range(NX):
             message = values[xt * R : (xt + 1) * R]
             for at, piece in enumerate(split3(totals[:, xt : xt + 1])):
@@ -188,8 +203,8 @@
         for dx in (1, 3, 2, 0):
             read_copy((xm + dx) % NX, xm).start()
 
-    wk_copy.wait()
-    wv_copy.wait()
+    for copy in weights:
+        copy.wait()
     low_half = lax.broadcasted_iota(jnp.int32, (ROWS, LANES), 1) < HD
 
     def project(k, c):
@@ -213,6 +228,10 @@
             for dx in range(NX):
                 query_copy((xm + dx) % NX, xm).start()
 
+        @pl.when(k == LAST)
+        def _():
+            read_at_source()
+
         @pl.when(k != LAST)
         def _():
             send_plane(k)
@@ -220,6 +239,7 @@
         return c
 
     lax.fori_loop(0, NZ, project, 0)
+    send_plane(LAST)
 
     for xt in range(NX):
         @pl.when(xt == xm)
@@ -239,29 +259,32 @@
             device_id_type=MESH,
         )
 
-    def read_plane(k, total):
+    def read_plane(at, c):
+        k = at + jnp.where(at < LAST, 0, 1)
         zs = (z - plane_offset(k) + NZ) % NZ
+
+        @pl.when(at == NZ - 2)
+        def _():
+            for xs in range(NX):
+                read_copy(xs, xs).wait_recv()
+                message = tv_in[xs].astype(jnp.float32)
+                sums = message[:, 0:1] + message[:, 1:2] + message[:, 2:3]
+                tots[...] += jnp.where(lane == far * NX + xs, sums, 0.0)
+                vals[far * NX + xs] = message
+
         for xs in range(NX):
             @pl.when(jnp.logical_or(k != OWN, xs != xm))
             def _():
                 arrival(k, xs).wait_recv()
         rows = [land[p, pl.ds(zs * NX, NX)].reshape(PLANE, LANES) for p in range(PAIRS)]
         totals, values = read(rows, qc[...], own_bias, zs * NX)
+        tots[...] += totals
         for b in range(NX):
             vals[zs * NX + b] = values[b * R : (b + 1) * R]
-        return total + totals
-
-    total = jnp.zeros((R, LANES), jnp.float32)
-    total = lax.fori_loop(0, FIRST_READS, read_plane, total)
-    read_at_source()
-    send_plane(LAST)
-    total = lax.fori_loop(FIRST_READS, LAST, read_plane, total)
-    for xs in range(NX):
-        read_copy(xs, xs).wait_recv()
-        message = tv_in[xs].astype(jnp.float32)
-        sums = message[:, 0:1] + message[:, 1:2] + message[:, 2:3]
-        total = total + jnp.where(lane == far * NX + xs, sums, 0.0)
-        vals[far * NX + xs] = message
+        return c
+
+    tots[...] = jnp.zeros((R, LANES), jnp.float32)
+    lax.fori_loop(0, NZ - 1, read_plane, 0)
 
     def exchange(src, dst, ssem, rsem):
         return [
@@ -272,14 +295,13 @@
             for i in range(1, NTP)
         ]
 
-    tots[...] = total
     copies = exchange(tots, tot_in, tsend, trecv)
     for copy in copies:
         copy.start()
     for copy in copies:
         copy.wait()
-    every = total
-    inside_later = jnp.zeros_like(total)
+    every = tots[...]
+    inside_later = jnp.zeros_like(every)
     for i in range(1, NTP):
         other = tot_in[i]
         every = every + other
@@ -295,11 +317,6 @@
     copies = exchange(part, part_in, psend, precv)
     for copy in copies:
         copy.start()
-    for copy in copies:
-        copy.wait()
-    for i in range(1, NTP):
-        partial = partial + part_in[i]
-    usum[...] = partial
 
     for xs in range(NX):
         arrival(LAST, xs).wait_recv()
@@ -316,10 +333,25 @@
         query_copy(xt, xt).wait_send()
         read_copy(xt, xt).wait_send()
 
-
-def finish_kernel(land, usum, stored, first_read, fr_v, out_sem):
-    copy = pltpu.make_async_copy(land, stored, out_sem.at[0])
-    copy.start()
+    for copy in copies:
+        copy.wait()
+    for i in range(1, NTP):
+        partial = partial + part_in[i]
+    usum[...] = partial
+
+
+def finish_kernel(land, usum, stored, first_read, fr_v, fr_b, out_sem, fr_sem):
+    copies = [
+        pltpu.make_async_copy(
+            land.at[p, pl.ds(half * NSP // 4, NSP // 4)],
+            stored.at[p, pl.ds(half * NSP // 4, NSP // 4)],
+            out_sem.at[p, half],
+        )
+        for p in range(PAIRS)
+        for half in range(4)
+    ]
+    for copy in copies:
+        copy.start()
     summed = usum[...]
     lane = lax.broadcasted_iota(jnp.int32, (R, LANES), 1)
     summed = jnp.where(lane >= HD, summed, 0.0)
@@ -333,8 +365,12 @@
             fr_v[p : p + 1, g * HD : (g + 1) * HD] = source[
                 p * GROUP + g : p * GROUP + g + 1, lo : lo + HD
             ]
-    first_read[...] = fr_v[...].astype(jnp.bfloat16)
-    copy.wait()
+    fr_b[...] = fr_v[...].astype(jnp.bfloat16)
+    fr_copy = pltpu.make_async_copy(fr_b, first_read, fr_sem.at[0])
+    fr_copy.start()
+    for copy in copies:
+        copy.wait()
+    fr_copy.wait()
 
 
 def per_device(layer_input, key_weight, value_weight, queries, head_bias):
@@ -362,11 +398,13 @@
             pltpu.VMEM((R, LANES), jnp.float32),
             pltpu.VMEM((NTP, R, LANES), jnp.float32),
             pltpu.VMEM((NTP, R, LANES), jnp.float32),
-            pltpu.VMEM((NX, R, LANES), jnp.bfloat16),
+            pltpu.VMEM((R // 2, LANES), jnp.bfloat16),
+            pltpu.VMEM((NX, R // 2, LANES), jnp.bfloat16),
             pltpu.VMEM((NX, R, LANES), jnp.bfloat16),
             pltpu.VMEM((NX, R, LANES), jnp.bfloat16),
             pltpu.SemaphoreType.DMA((NZ,)),
-            pltpu.SemaphoreType.DMA((4,)),
+            pltpu.SemaphoreType.DMA((2 * CUTS,)),
+            pltpu.SemaphoreType.DMA((2,)),
             pltpu.SemaphoreType.DMA((NZ, NX)),
             pltpu.SemaphoreType.DMA((NZ, NX)),
             pltpu.SemaphoreType.DMA((NTP,)),
@@ -379,10 +417,17 @@
             pltpu.SemaphoreType.DMA((NX,)),
         ],
         compiler_params=pltpu.CompilerParams(
-            collective_id=0, has_side_effects=True, vmem_limit_bytes=53672 * 1024
+            collective_id=0, has_side_effects=True, vmem_limit_bytes=40 * 1024 * 1024
         ),
         name="project_exchange_read",
-    )(layer_input, key_weight, value_weight, queries.transpose(1, 0, 2), head_bias)
+    )(
+        *(
+            pltpu.with_memory_space_constraint(operand, pltpu.HBM)
+            for operand in (
+                layer_input, key_weight, value_weight, queries.transpose(1, 0, 2), head_bias
+            )
+        )
+    )
     stored, first_read = pl.pallas_call(
         finish_kernel,
         out_shape=(
@@ -390,9 +435,11 @@
             jax.ShapeDtypeStruct((PAIRS, GROUP * HD), jnp.bfloat16),
         ),
         in_specs=[pl.BlockSpec(memory_space=pl.ANY), vmem],
-        out_specs=(pl.BlockSpec(memory_space=pl.ANY), vmem),
+        out_specs=(pl.BlockSpec(memory_space=pl.ANY), pl.BlockSpec(memory_space=pl.ANY)),
         scratch_shapes=[
             pltpu.VMEM((PAIRS, GROUP * HD), jnp.float32),
+            pltpu.VMEM((PAIRS, GROUP * HD), jnp.bfloat16),
+            pltpu.SemaphoreType.DMA((PAIRS, 4)),
             pltpu.SemaphoreType.DMA((1,)),
         ],
         compiler_params=pltpu.CompilerParams(vmem_limit_bytes=8 * 1024 * 1024),

time: 57 us -> 53.8 us (0.944)
  Pallas kernels: 54.8 us -> 53.1 us
  local copies, waits for them, and re-layouts: 1.37 us -> 0 us
    unnamed x4 -> x0, local copies, waits for them, and re-layouts: 1.37 us -> none
    pallas_call x1, Pallas kernels: 53.1 us -> 51.9 us  [per_device(): pl.pallas_call(main_kernel, out_shape=(jax.ShapeDtypeStruct((PAIRS, NSP,...]
where the time goes in v3:
time: 53.8 us
  Pallas kernels  53.1 us (99%)
  between operations  0.64 us (1%)
    pallas_call x1, Pallas kernels, per_device(): pl.pallas_call(main_kernel, out_shape=(jax.ShapeDtypeStruct((PAIRS, NSP,...  51.9 us
    pallas_call x1, Pallas kernels, per_device(): pl.pallas_call(finish_kernel, out_shape=(jax.ShapeDtypeStruct(land.shape,...  1.25 us

profile of v3, /device:TPU:1, one launch (start us, length us, event | category | flops | bytes accessed | tf_op | source)
XLA Modules:
  0.0 53.8 jit_solution(3886960833490303634)
XLA Ops:
  0.6 51.9 %project_exchange_read.1 = (bf16[3,32,64,128]{3,2,1,0:T(8,128)(2,1)S(1)}, f32[16,128]{1,0:T(8,128)S(1)}) custom-call(bf16[16,64,2048]{2,1,0:T(8,128)(2,1)} %x_hbm.1, bf16[2048,384]{1,0:T(8,128)(2,1)} %wk_hbm.1, bf16[2048,384]{1,0:T(8,128)(2,1)} %wv_hbm.1, bf16[5,3,64]{2,1,0:T(4,128)(2,1)} %bitcast.1, f32[6,5]{1,0:T(8,128)} %bias_hbm.1), custom_call_target="tpu_custom_call" | custom-call | tf_op jit(solution)/shard_map/project_exchange_read/pallas_call | solution.py:380
  52.5 1.2 %finish.1 = (bf16[3,32,64,128]{3,2,1,0:T(8,128)(2,1)}, bf16[3,320]{1,0:T(4,128)(2,1)}) custom-call(bf16[3,32,64,128]{3,2,1,0:T(8,128)(2,1)S(1)} %get-tuple-element.4.land, f32[16,128]{1,0:T(8,128)S(1)} %get-tuple-element.5.usum), custom_call_target="tpu_custom_call" | custom-call | tf_op jit(solution)/shard_map/finish/pallas_call | solution.py:431

commit v4 on v3

--- a/solution.py
+++ b/solution.py
@@ -66,16 +66,16 @@
         zt = (z + plane_offset(k)) % NZ
         return pltpu.make_async_copy(x_hbm.at[pl.ds(2 * zt, 2)], x_v.at[k], x_sem.at[k])
 
-    def weight_copies(w_hbm, w_v, first):
+    def weight_copies(w_hbm, w_v, which):
         part = w_v.shape[0] // CUTS
         return [
             pltpu.make_async_copy(
-                w_hbm.at[pl.ds(i * part, part)], w_v.at[pl.ds(i * part, part)], w_sem.at[first + i]
+                w_hbm.at[pl.ds(i * part, part)], w_v.at[pl.ds(i * part, part)], w_sem.at[which]
             )
             for i in range(CUTS)
         ]
 
-    weights = weight_copies(wk_hbm, wk_v, 0) + weight_copies(wv_hbm, wv_v, CUTS)
+    weights = weight_copies(wk_hbm, wk_v, 0) + weight_copies(wv_hbm, wv_v, 1)
     q_copy = pltpu.make_async_copy(q_hbm, q_v, in_sem.at[0])
     bias_copy = pltpu.make_async_copy(bias_hbm, bias_s, in_sem.at[1])
     x_copy(0).start()
@@ -101,10 +101,16 @@
         return pltpu.make_async_remote_copy(
             src_ref=stage.at[k, xt],
             dst_ref=land.at[:, sp],
-            send_sem=send_sem.at[k, xt],
-            recv_sem=recv_sem.at[k, xm],
+            send_sem=send_sem.at[k],
+            recv_sem=recv_sem.at[k],
             device_id={"sp": zt * NX + xt},
             device_id_type=MESH,
+        )
+
+    def group(ref, ssem, rsem):
+        return pltpu.make_async_remote_copy(
+            src_ref=ref, dst_ref=ref, send_sem=ssem, recv_sem=rsem,
+            device_id={"sp": sp}, device_id_type=MESH,
         )
 
     def send_plane(k):
@@ -173,20 +179,19 @@
 
     def query_copy(xt, slot):
         return pltpu.make_async_remote_copy(
-            src_ref=q_out, dst_ref=q_in.at[slot], send_sem=qsend.at[xt], recv_sem=qrecv.at[slot],
+            src_ref=q_out, dst_ref=q_in.at[slot], send_sem=qsend, recv_sem=qrecv,
             device_id={"sp": far * NX + xt}, device_id_type=MESH,
         )
 
     def read_copy(xt, slot):
         return pltpu.make_async_remote_copy(
             src_ref=tv_out.at[xt], dst_ref=tv_in.at[slot],
-            send_sem=vsend.at[xt], recv_sem=vrecv.at[slot],
+            send_sem=vsend, recv_sem=vrecv,
             device_id={"sp": far * NX + xt}, device_id_type=MESH,
         )
 
     def read_at_source():
-        for xt in range(NX):
-            query_copy(xt, xt).wait_recv()
+        group(q_in, qsend, qrecv).wait_recv()
         rows = [stage[LAST, :, p].reshape(PLANE, LANES) for p in range(PAIRS)]
         low = lane[: R // 2] < HD
         pieces = []
@@ -203,8 +208,8 @@
         for dx in (1, 3, 2, 0):
             read_copy((xm + dx) % NX, xm).start()
 
-    for copy in weights:
-        copy.wait()
+    pltpu.make_async_copy(wk_hbm, wk_v, w_sem.at[0]).wait()
+    pltpu.make_async_copy(wv_hbm, wv_v, w_sem.at[1]).wait()
     low_half = lax.broadcasted_iota(jnp.int32, (ROWS, LANES), 1) < HD
 
     def project(k, c):
@@ -239,7 +244,10 @@
         return c
 
     lax.fori_loop(0, NZ, project, 0)
-    send_plane(LAST)
+
+    @pl.when(tp % 2 == 0)
+    def _():
+        send_plane(LAST)
 
     for xt in range(NX):
         @pl.when(xt == xm)
@@ -248,16 +256,10 @@
 
     own_bias = bias_table(sp % 2 == 1)
 
-    def arrival(k, xs):
-        zs = (z - plane_offset(k) + NZ) % NZ
-        return pltpu.make_async_remote_copy(
-            src_ref=stage.at[k, xs],
-            dst_ref=land.at[:, zs * NX + xs],
-            send_sem=send_sem.at[k, xs],
-            recv_sem=recv_sem.at[k, xs],
-            device_id={"sp": zs * NX + xs},
-            device_id_type=MESH,
-        )
+    def arrival(zs, k):
+        return group(land.at[:, pl.ds(zs * NX, NX)], send_sem.at[k], recv_sem.at[k])
+
+    own_group = group(land.at[:, pl.ds(0, NX - 1)], send_sem.at[OWN], recv_sem.at[OWN])
 
     def read_plane(at, c):
         k = at + jnp.where(at < LAST, 0, 1)
@@ -265,17 +267,25 @@
 
         @pl.when(at == NZ - 2)
         def _():
+            group(tv_in, vsend, vrecv).wait_recv()
             for xs in range(NX):
-                read_copy(xs, xs).wait_recv()
                 message = tv_in[xs].astype(jnp.float32)
                 sums = message[:, 0:1] + message[:, 1:2] + message[:, 2:3]
                 tots[...] += jnp.where(lane == far * NX + xs, sums, 0.0)
                 vals[far * NX + xs] = message
 
-        for xs in range(NX):
-            @pl.when(jnp.logical_or(k != OWN, xs != xm))
-            def _():
-                arrival(k, xs).wait_recv()
+        @pl.when(k != OWN)
+        def _():
+            arrival(zs, k).wait_recv()
+
+        @pl.when(k == OWN)
+        def _():
+            own_group.wait_recv()
+
+        @pl.when(jnp.logical_and(at == NZ - 2, tp % 2 == 1))
+        def _():
+            send_plane(LAST)
+
         rows = [land[p, pl.ds(zs * NX, NX)].reshape(PLANE, LANES) for p in range(PAIRS)]
         totals, values = read(rows, qc[...], own_bias, zs * NX)
         tots[...] += totals
@@ -289,7 +299,7 @@
     def exchange(src, dst, ssem, rsem):
         return [
             pltpu.make_async_remote_copy(
-                src_ref=src, dst_ref=dst.at[i], send_sem=ssem.at[i], recv_sem=rsem.at[i],
+                src_ref=src, dst_ref=dst.at[i], send_sem=ssem, recv_sem=rsem,
                 device_id={"tp": (tp + i) % NTP}, device_id_type=MESH,
             )
             for i in range(1, NTP)
@@ -298,8 +308,7 @@
     copies = exchange(tots, tot_in, tsend, trecv)
     for copy in copies:
         copy.start()
-    for copy in copies:
-        copy.wait()
+    group(tot_in.at[pl.ds(1, NTP - 1)], tsend, trecv).wait()
     every = tots[...]
     inside_later = jnp.zeros_like(every)
     for i in range(1, NTP):
@@ -318,23 +327,16 @@
     for copy in copies:
         copy.start()
 
-    for xs in range(NX):
-        arrival(LAST, xs).wait_recv()
-
-    def drain(k, c):
-        for xt in range(NX):
-            @pl.when(jnp.logical_or(k != OWN, xt != xm))
-            def _():
-                block_copy(k, xt).wait_send()
-        return c
-
-    lax.fori_loop(0, NZ, drain, 0)
-    for xt in range(NX):
-        query_copy(xt, xt).wait_send()
-        read_copy(xt, xt).wait_send()
-
-    for copy in copies:
-        copy.wait()
+    arrival(far, LAST).wait_recv()
+    for k in range(NZ):
+        if k == OWN:
+            own_group.wait_send()
+        else:
+            group(stage.at[k], send_sem.at[k], recv_sem.at[k]).wait_send()
+    group(q_in, qsend, qrecv).wait_send()
+    group(tv_in, vsend, vrecv).wait_send()
+
+    group(part_in.at[pl.ds(1, NTP - 1)], psend, precv).wait()
     for i in range(1, NTP):
         partial = partial + part_in[i]
     usum[...] = partial
@@ -403,18 +405,18 @@
             pltpu.VMEM((NX, R, LANES), jnp.bfloat16),
             pltpu.VMEM((NX, R, LANES), jnp.bfloat16),
             pltpu.SemaphoreType.DMA((NZ,)),
-            pltpu.SemaphoreType.DMA((2 * CUTS,)),
             pltpu.SemaphoreType.DMA((2,)),
-            pltpu.SemaphoreType.DMA((NZ, NX)),
-            pltpu.SemaphoreType.DMA((NZ, NX)),
-            pltpu.SemaphoreType.DMA((NTP,)),
-            pltpu.SemaphoreType.DMA((NTP,)),
-            pltpu.SemaphoreType.DMA((NTP,)),
-            pltpu.SemaphoreType.DMA((NTP,)),
-            pltpu.SemaphoreType.DMA((NX,)),
-            pltpu.SemaphoreType.DMA((NX,)),
-            pltpu.SemaphoreType.DMA((NX,)),
-            pltpu.SemaphoreType.DMA((NX,)),
+            pltpu.SemaphoreType.DMA((2,)),
+            pltpu.SemaphoreType.DMA((NZ,)),
+            pltpu.SemaphoreType.DMA((NZ,)),
+            pltpu.SemaphoreType.DMA,
+            pltpu.SemaphoreType.DMA,
+            pltpu.SemaphoreType.DMA,
+            pltpu.SemaphoreType.DMA,
+            pltpu.SemaphoreType.DMA,
+            pltpu.SemaphoreType.DMA,
+            pltpu.SemaphoreType.DMA,
+            pltpu.SemaphoreType.DMA,
         ],
         compiler_params=pltpu.CompilerParams(
             collective_id=0, has_side_effects=True, vmem_limit_bytes=40 * 1024 * 1024

time: 53.8 us -> 52.1 us (0.968)
  Pallas kernels: 53.1 us -> 51.4 us
    pallas_call x1, Pallas kernels: 51.9 us -> 50.1 us  [per_device(): pl.pallas_call(main_kernel, out_shape=(jax.ShapeDtypeStruct((PAIRS, NSP,...]
where the time goes in v4:
time: 52.1 us; the launch traced here: 52 us
  Pallas kernels  51.4 us (99%)
  between operations  0.64 us (1%)
    pallas_call x1, Pallas kernels, per_device(): pl.pallas_call(main_kernel, out_shape=(jax.ShapeDtypeStruct((PAIRS, NSP,...  50.1 us
    pallas_call x1, Pallas kernels, per_device(): pl.pallas_call(finish_kernel, out_shape=(jax.ShapeDtypeStruct(land.shape,...  1.25 us

profile of v4, /device:TPU:1, one launch (start us, length us, event | category | flops | bytes accessed | tf_op | source)
XLA Modules:
  0.0 52.0 jit_solution(16176468328192961491)
XLA Ops:
  0.6 50.1 %project_exchange_read.1 = (bf16[3,32,64,128]{3,2,1,0:T(8,128)(2,1)S(1)}, f32[16,128]{1,0:T(8,128)S(1)}) custom-call(bf16[16,64,2048]{2,1,0:T(8,128)(2,1)} %x_hbm.1, bf16[2048,384]{1,0:T(8,128)(2,1)} %wk_hbm.1, bf16[2048,384]{1,0:T(8,128)(2,1)} %wv_hbm.1, bf16[5,3,64]{2,1,0:T(4,128)(2,1)} %bitcast.1, f32[6,5]{1,0:T(8,128)} %bias_hbm.1), custom_call_target="tpu_custom_call" | custom-call | tf_op jit(solution)/shard_map/project_exchange_read/pallas_call | solution.py:382
  50.8 1.2 %finish.1 = (bf16[3,32,64,128]{3,2,1,0:T(8,128)(2,1)}, bf16[3,320]{1,0:T(4,128)(2,1)}) custom-call(bf16[3,32,64,128]{3,2,1,0:T(8,128)(2,1)S(1)} %get-tuple-element.4.land, f32[16,128]{1,0:T(8,128)S(1)} %get-tuple-element.5.usum), custom_call_target="tpu_custom_call" | custom-call | tf_op jit(solution)/shard_map/finish/pallas_call | solution.py:433

commit v5 on v4

--- a/solution.py
+++ b/solution.py
@@ -62,6 +62,16 @@
     z = sp // NX
     xm = sp % NX
 
+    barrier = pltpu.get_barrier_semaphore()
+    for i in range(1, NSP):
+        pl.semaphore_signal(
+            barrier, 1, device_id={"sp": (sp + i) % NSP}, device_id_type=MESH
+        )
+    for i in range(1, NTP):
+        pl.semaphore_signal(
+            barrier, 1, device_id={"tp": (tp + i) % NTP}, device_id_type=MESH
+        )
+
     def x_copy(k):
         zt = (z + plane_offset(k)) % NZ
         return pltpu.make_async_copy(x_hbm.at[pl.ds(2 * zt, 2)], x_v.at[k], x_sem.at[k])
@@ -83,18 +93,7 @@
         copy.start()
     q_copy.start()
     bias_copy.start()
-    for k in range(1, NZ):
-        x_copy(k).start()
-
-    barrier = pltpu.get_barrier_semaphore()
-    for i in range(1, NSP):
-        pl.semaphore_signal(
-            barrier, 1, device_id={"sp": (sp + i) % NSP}, device_id_type=MESH
-        )
-    for i in range(1, NTP):
-        pl.semaphore_signal(
-            barrier, 1, device_id={"tp": (tp + i) % NTP}, device_id_type=MESH
-        )
+    x_copy(1).start()
 
     def block_copy(k, xt):
         zt = (z + plane_offset(k)) % NZ
@@ -139,7 +138,7 @@
                 table = jnp.where(row == p * GROUP + g, value, table)
         return table
 
-    def read(rows, query, bias, first):
+    def read(rows, query, bias, first, with_totals=lambda totals: None):
         scores = jnp.zeros((R, PLANE), jnp.float32)
         for p in range(PAIRS):
             dots = lax.dot_general(
@@ -156,6 +155,7 @@
         pick = jnp.where(blk_i + first == blk_j, 1.0, 0.0).astype(jnp.bfloat16)
         sums = exact_dot(keep, jnp.concatenate([later, pick], axis=1))
         inside, totals = sums[:, :PLANE], sums[:, PLANE:]
+        with_totals(totals)
         weights = jnp.exp(scores + keep + inside)
         spread = jnp.concatenate(
             [jnp.where(lane_blk == b, weights, 0.0) for b in range(NX)], axis=0
@@ -210,6 +210,8 @@
 
     pltpu.make_async_copy(wk_hbm, wk_v, w_sem.at[0]).wait()
     pltpu.make_async_copy(wv_hbm, wv_v, w_sem.at[1]).wait()
+    for k in range(2, NZ):
+        x_copy(k).start()
     low_half = lax.broadcasted_iota(jnp.int32, (ROWS, LANES), 1) < HD
 
     def project(k, c):
@@ -261,9 +263,23 @@
 
     own_group = group(land.at[:, pl.ds(0, NX - 1)], send_sem.at[OWN], recv_sem.at[OWN])
 
+    half = R // 2
+    lane8 = lane[:half]
+
+    def exchange(src, dst, ssem, rsem):
+        for i in (4, 3, 5, 2, 6, 1, 7):
+            pltpu.make_async_remote_copy(
+                src_ref=src, dst_ref=dst.at[i], send_sem=ssem, recv_sem=rsem,
+                device_id={"tp": (tp + i) % NTP}, device_id_type=MESH,
+            ).start()
+
     def read_plane(at, c):
         k = at + jnp.where(at < LAST, 0, 1)
         zs = (z - plane_offset(k) + NZ) % NZ
+
+        @pl.when(jnp.logical_and(at == NZ - 2, tp % 2 == 1))
+        def _():
+            send_plane(LAST)
 
         @pl.when(at == NZ - 2)
         def _():
@@ -271,7 +287,8 @@
             for xs in range(NX):
                 message = tv_in[xs].astype(jnp.float32)
                 sums = message[:, 0:1] + message[:, 1:2] + message[:, 2:3]
-                tots[...] += jnp.where(lane == far * NX + xs, sums, 0.0)
+                sums = jnp.where(lane == far * NX + xs, sums, 0.0)
+                tots[...] += sums[:half] + pltpu.roll(sums[half:], NSP, 1)
                 vals[far * NX + xs] = message
 
         @pl.when(k != OWN)
@@ -282,32 +299,23 @@
         def _():
             own_group.wait_recv()
 
-        @pl.when(jnp.logical_and(at == NZ - 2, tp % 2 == 1))
-        def _():
-            send_plane(LAST)
-
         rows = [land[p, pl.ds(zs * NX, NX)].reshape(PLANE, LANES) for p in range(PAIRS)]
-        totals, values = read(rows, qc[...], own_bias, zs * NX)
-        tots[...] += totals
+
+        def add_totals(totals):
+            tots[...] += totals[:half] + pltpu.roll(totals[half:], NSP, 1)
+
+            @pl.when(at == NZ - 2)
+            def _():
+                exchange(tots, tot_in, tsend, trecv)
+
+        totals, values = read(rows, qc[...], own_bias, zs * NX, add_totals)
         for b in range(NX):
             vals[zs * NX + b] = values[b * R : (b + 1) * R]
         return c
 
-    tots[...] = jnp.zeros((R, LANES), jnp.float32)
+    tots[...] = jnp.zeros((half, LANES), jnp.float32)
     lax.fori_loop(0, NZ - 1, read_plane, 0)
 
-    def exchange(src, dst, ssem, rsem):
-        return [
-            pltpu.make_async_remote_copy(
-                src_ref=src, dst_ref=dst.at[i], send_sem=ssem, recv_sem=rsem,
-                device_id={"tp": (tp + i) % NTP}, device_id_type=MESH,
-            )
-            for i in range(1, NTP)
-        ]
-
-    copies = exchange(tots, tot_in, tsend, trecv)
-    for copy in copies:
-        copy.start()
     group(tot_in.at[pl.ds(1, NTP - 1)], tsend, trecv).wait()
     every = tots[...]
     inside_later = jnp.zeros_like(every)
@@ -315,6 +323,12 @@
         other = tot_in[i]
         every = every + other
         inside_later = inside_later + jnp.where(tp - i < 0, other, 0.0)
+    def one_below_other(packed):
+        low = lane8 < NSP
+        above, under = packed, pltpu.roll(packed, LANES - NSP, 1)
+        return jnp.concatenate([jnp.where(low, above, 0.0), jnp.where(low, under, 0.0)], axis=0)
+
+    every, inside_later = one_below_other(every), one_below_other(inside_later)
     chunk_i = lax.broadcasted_iota(jnp.int32, (LANES, LANES), 0)
     chunk_j = lax.broadcasted_iota(jnp.int32, (LANES, LANES), 1)
     after = jnp.where(chunk_i > chunk_j, 1.0, 0.0).astype(jnp.bfloat16)
@@ -322,10 +336,9 @@
     partial = jnp.zeros((R, LANES), jnp.float32)
     for b in range(NSP):
         partial = partial + scale[:, b : b + 1] * vals[b]
+    partial = jnp.where(lane8 < HD, pltpu.roll(partial[half:], HD, 1), partial[:half])
     part[...] = partial
-    copies = exchange(part, part_in, psend, precv)
-    for copy in copies:
-        copy.start()
+    exchange(part, part_in, psend, precv)
 
     arrival(far, LAST).wait_recv()
     for k in range(NZ):
@@ -339,7 +352,7 @@
     group(part_in.at[pl.ds(1, NTP - 1)], psend, precv).wait()
     for i in range(1, NTP):
         partial = partial + part_in[i]
-    usum[...] = partial
+    usum[...] = jnp.concatenate([partial, pltpu.roll(partial, HD, 1)], axis=0)
 
 
 def finish_kernel(land, usum, stored, first_read, fr_v, fr_b, out_sem, fr_sem):
@@ -396,10 +409,10 @@
             pltpu.SMEM(head_bias.shape, jnp.float32),
             pltpu.VMEM((NZ, NX, PAIRS, ROWS, LANES), jnp.bfloat16),
             pltpu.VMEM((NSP, R, LANES), jnp.float32),
-            pltpu.VMEM((R, LANES), jnp.float32),
-            pltpu.VMEM((R, LANES), jnp.float32),
-            pltpu.VMEM((NTP, R, LANES), jnp.float32),
-            pltpu.VMEM((NTP, R, LANES), jnp.float32),
+            pltpu.VMEM((R // 2, LANES), jnp.float32),
+            pltpu.VMEM((R // 2, LANES), jnp.float32),
+            pltpu.VMEM((NTP, R // 2, LANES), jnp.float32),
+            pltpu.VMEM((NTP, R // 2, LANES), jnp.float32),
             pltpu.VMEM((R // 2, LANES), jnp.bfloat16),
             pltpu.VMEM((NX, R // 2, LANES), jnp.bfloat16),
             pltpu.VMEM((NX, R, LANES), jnp.bfloat16),

time: 52.1 us -> 51.6 us (level)
  no operation moved by 1% of the time
where the time goes in v5:
time: 51.6 us; the launch traced here: 51.5 us
  Pallas kernels  50.9 us (99%)
  between operations  0.64 us (1%)
    pallas_call x1, Pallas kernels, per_device(): pl.pallas_call(main_kernel, out_shape=(jax.ShapeDtypeStruct((PAIRS, NSP,...  49.6 us
    pallas_call x1, Pallas kernels, per_device(): pl.pallas_call(finish_kernel, out_shape=(jax.ShapeDtypeStruct(land.shape,...  1.25 us

profile of v5, /device:TPU:1, one launch (start us, length us, event | category | flops | bytes accessed | tf_op | source)
XLA Modules:
  0.0 51.5 jit_solution(10527614008851986266)
XLA Ops:
  0.6 49.6 %project_exchange_read.1 = (bf16[3,32,64,128]{3,2,1,0:T(8,128)(2,1)S(1)}, f32[16,128]{1,0:T(8,128)S(1)}) custom-call(bf16[16,64,2048]{2,1,0:T(8,128)(2,1)} %x_hbm.1, bf16[2048,384]{1,0:T(8,128)(2,1)} %wk_hbm.1, bf16[2048,384]{1,0:T(8,128)(2,1)} %wv_hbm.1, bf16[5,3,64]{2,1,0:T(4,128)(2,1)} %bitcast.1, f32[6,5]{1,0:T(8,128)} %bias_hbm.1), custom_call_target="tpu_custom_call" | custom-call | tf_op jit(solution)/shard_map/project_exchange_read/pallas_call | solution.py:395
  50.3 1.2 %finish.1 = (bf16[3,32,64,128]{3,2,1,0:T(8,128)(2,1)}, bf16[3,320]{1,0:T(4,128)(2,1)}) custom-call(bf16[3,32,64,128]{3,2,1,0:T(8,128)(2,1)S(1)} %get-tuple-element.4.land, f32[16,128]{1,0:T(8,128)S(1)} %get-tuple-element.5.usum), custom_call_target="tpu_custom_call" | custom-call | tf_op jit(solution)/shard_map/finish/pallas_call | solution.py:446

commit v6 on v5

--- a/solution.py
+++ b/solution.py
@@ -23,7 +23,7 @@
 R = 16
 PLANE = NX * ROWS
 CUTS = 4
-ORDER = (1, 7, 0, 2, 6, 4, 3, 5)
+ORDER = (2, 6, 0, 3, 5, 4, 1, 7)
 OWN = ORDER.index(0)
 LAST = ORDER.index(NZ // 2)
 
@@ -62,16 +62,6 @@
     z = sp // NX
     xm = sp % NX
 
-    barrier = pltpu.get_barrier_semaphore()
-    for i in range(1, NSP):
-        pl.semaphore_signal(
-            barrier, 1, device_id={"sp": (sp + i) % NSP}, device_id_type=MESH
-        )
-    for i in range(1, NTP):
-        pl.semaphore_signal(
-            barrier, 1, device_id={"tp": (tp + i) % NTP}, device_id_type=MESH
-        )
-
     def x_copy(k):
         zt = (z + plane_offset(k)) % NZ
         return pltpu.make_async_copy(x_hbm.at[pl.ds(2 * zt, 2)], x_v.at[k], x_sem.at[k])
@@ -91,6 +81,17 @@
     x_copy(0).start()
     for copy in weights:
         copy.start()
+
+    barrier = pltpu.get_barrier_semaphore()
+    for i in range(1, NSP):
+        pl.semaphore_signal(
+            barrier, 1, device_id={"sp": (sp + i) % NSP}, device_id_type=MESH
+        )
+    for i in range(1, NTP):
+        pl.semaphore_signal(
+            barrier, 1, device_id={"tp": (tp + i) % NTP}, device_id_type=MESH
+        )
+
     q_copy.start()
     bias_copy.start()
     x_copy(1).start()

time: 51.6 us -> 50.7 us (0.983)
  Pallas kernels: 50.9 us -> 49.9 us
    pallas_call x1, Pallas kernels: 49.6 us -> 48.6 us  [per_device(): pl.pallas_call(main_kernel, out_shape=(jax.ShapeDtypeStruct((PAIRS, NSP,...]
where the time goes in v6:
time: 50.7 us; the launch traced here: 50.5 us
  Pallas kernels  49.9 us (98%)
  between operations  0.64 us (1%)
    pallas_call x1, Pallas kernels, per_device(): pl.pallas_call(main_kernel, out_shape=(jax.ShapeDtypeStruct((PAIRS, NSP,...  48.6 us
    pallas_call x1, Pallas kernels, per_device(): pl.pallas_call(finish_kernel, out_shape=(jax.ShapeDtypeStruct(land.shape,...  1.25 us

profile of v6, /device:TPU:1, one launch (start us, length us, event | category | flops | bytes accessed | tf_op | source)
XLA Modules:
  0.0 50.5 jit_solution(12088396878337740989)
XLA Ops:
  0.6 48.6 %project_exchange_read.1 = (bf16[3,32,64,128]{3,2,1,0:T(8,128)(2,1)S(1)}, f32[16,128]{1,0:T(8,128)S(1)}) custom-call(bf16[16,64,2048]{2,1,0:T(8,128)(2,1)} %x_hbm.1, bf16[2048,384]{1,0:T(8,128)(2,1)} %wk_hbm.1, bf16[2048,384]{1,0:T(8,128)(2,1)} %wv_hbm.1, bf16[5,3,64]{2,1,0:T(4,128)(2,1)} %bitcast.1, f32[6,5]{1,0:T(8,128)} %bias_hbm.1), custom_call_target="tpu_custom_call" | custom-call | tf_op jit(solution)/shard_map/project_exchange_read/pallas_call | solution.py:396
  49.3 1.2 %finish.1 = (bf16[3,32,64,128]{3,2,1,0:T(8,128)(2,1)}, bf16[3,320]{1,0:T(4,128)(2,1)}) custom-call(bf16[3,32,64,128]{3,2,1,0:T(8,128)(2,1)S(1)} %get-tuple-element.4.land, f32[16,128]{1,0:T(8,128)S(1)} %get-tuple-element.5.usum), custom_call_target="tpu_custom_call" | custom-call | tf_op jit(solution)/shard_map/finish/pallas_call | solution.py:447

commit v7 on v6

--- a/solution.py
+++ b/solution.py
@@ -167,15 +167,6 @@
             values = jnp.where(row_pair_v == p, out, values)
         return totals, values
 
-    q_copy.wait()
-    bias_copy.wait()
-    qc[...] = jnp.zeros_like(qc)
-    for p in range(PAIRS):
-        for g in range(GROUP):
-            qc[p * GROUP + g : p * GROUP + g + 1, 0:HD] = q_v[g, p : p + 1, :]
-    wide = qc[...].astype(jnp.float32)
-    q_out[...] = (wide[: R // 2] + pltpu.roll(wide[R // 2 :], HD, 1)).astype(jnp.bfloat16)
-
     far = (z + NZ // 2) % NZ
 
     def query_copy(xt, slot):
@@ -210,15 +201,19 @@
             read_copy((xm + dx) % NX, xm).start()
 
     pltpu.make_async_copy(wk_hbm, wk_v, w_sem.at[0]).wait()
-    pltpu.make_async_copy(wv_hbm, wv_v, w_sem.at[1]).wait()
-    for k in range(2, NZ):
-        x_copy(k).start()
     low_half = lax.broadcasted_iota(jnp.int32, (ROWS, LANES), 1) < HD
 
     def project(k, c):
         x_copy(k).wait()
         x = x_v[k].reshape(2 * ROWS, x_v.shape[-1])
         keys = jnp.dot(x, wk_v[...], preferred_element_type=jnp.float32)
+
+        @pl.when(k == 0)
+        def _():
+            pltpu.make_async_copy(wv_hbm, wv_v, w_sem.at[1]).wait()
+            for other in range(2, NZ):
+                x_copy(other).start()
+
         values = jnp.dot(x, wv_v[...], preferred_element_type=jnp.float32)
         for half in range(2):
             for pair in range(3):
@@ -232,6 +227,14 @@
 
         @pl.when(k == 0)
         def _():
+            q_copy.wait()
+            bias_copy.wait()
+            qc[...] = jnp.zeros_like(qc)
+            for p in range(PAIRS):
+                for g in range(GROUP):
+                    qc[p * GROUP + g : p * GROUP + g + 1, 0:HD] = q_v[g, p : p + 1, :]
+            wide = qc[...].astype(jnp.float32)
+            q_out[...] = (wide[: R // 2] + pltpu.roll(wide[R // 2 :], HD, 1)).astype(jnp.bfloat16)
             pl.semaphore_wait(barrier, NSP - 1 + NTP - 1)
             for dx in range(NX):
                 query_copy((xm + dx) % NX, xm).start()

time: 50.7 us -> 50.9 us (level)
  no operation moved by 1% of the time
where the time goes in v7:
time: 50.9 us; the launch traced here: 50.6 us
  Pallas kernels  50 us (98%)
  between operations  0.64 us (1%)
    pallas_call x1, Pallas kernels, per_device(): pl.pallas_call(main_kernel, out_shape=(jax.ShapeDtypeStruct((PAIRS, NSP,...  48.7 us
    pallas_call x1, Pallas kernels, per_device(): pl.pallas_call(finish_kernel, out_shape=(jax.ShapeDtypeStruct(land.shape,...  1.25 us

profile of v7, /device:TPU:1, one launch (start us, length us, event | category | flops | bytes accessed | tf_op | source)
XLA Modules:
  0.0 50.6 jit_solution(6512250818326267812)
XLA Ops:
  0.6 48.7 %project_exchange_read.1 = (bf16[3,32,64,128]{3,2,1,0:T(8,128)(2,1)S(1)}, f32[16,128]{1,0:T(8,128)S(1)}) custom-call(bf16[16,64,2048]{2,1,0:T(8,128)(2,1)} %x_hbm.1, bf16[2048,384]{1,0:T(8,128)(2,1)} %wk_hbm.1, bf16[2048,384]{1,0:T(8,128)(2,1)} %wv_hbm.1, bf16[5,3,64]{2,1,0:T(4,128)(2,1)} %bitcast.1, f32[6,5]{1,0:T(8,128)} %bias_hbm.1), custom_call_target="tpu_custom_call" | custom-call | tf_op jit(solution)/shard_map/project_exchange_read/pallas_call | solution.py:399
  49.4 1.2 %finish.1 = (bf16[3,32,64,128]{3,2,1,0:T(8,128)(2,1)}, bf16[3,320]{1,0:T(4,128)(2,1)}) custom-call(bf16[3,32,64,128]{3,2,1,0:T(8,128)(2,1)S(1)} %get-tuple-element.4.land, f32[16,128]{1,0:T(8,128)S(1)} %get-tuple-element.5.usum), custom_call_target="tpu_custom_call" | custom-call | tf_op jit(solution)/shard_map/finish/pallas_call | solution.py:450
